TPU v7x, 256 devices: a whole 4x4x8 slice. The times are simulated.
256 devices in a mesh: ep: 64 (over z, x, core), tp: 4 (over y).
Axes of the slice: x: 4, y: 4, z: 8, core: 2. Of those that a mesh axis runs over, the one named last changes fastest.
Arguments:
- conv_input: bfloat16 [65536, 2048], P('ep', 'tp'), may hold values from -6 to 6
- conv_kernel: bfloat16 [31, 2048], P(None, 'tp'), may hold values from -2 to 2
- norm_gain: float32 [2048], P('tp'), may hold values from 0.1 to 1.9
- norm_shift: float32 [2048], P('tp'), may hold values from -3 to 3
- conv_proj: bfloat16 [2048, 2048], P('tp'), may hold values from -0.125 to 0.125
- moe_input: bfloat16 [16384, 2048], P(('ep', 'tp')), may hold values from -6 to 6
- moe_gain: float32 [2048], replicated, may hold values from 0.1 to 1.9
- routes: int32 [16384, 2], P('ep'), may hold values from 0 to 63, all different within a row; in each aligned block of 256 rows (0 to 255, 256 to 511, ...) at most 16 rows name the same one
- route_weights: float32 [16384, 2], P('ep'), may hold values from 0.2 to 1
- gate_proj: bfloat16 [64, 2048, 2048], P('ep', None, 'tp'), may hold values from -0.125 to 0.125
- up_proj: bfloat16 [64, 2048, 2048], P('ep', None, 'tp'), may hold values from -0.125 to 0.125
- down_proj: bfloat16 [64, 2048, 2048], P('ep', 'tp'), may hold values from -0.125 to 0.125
Outputs:
- conv_out: bfloat16 [65536, 2048], P(('ep', 'tp'))
- moe_out: bfloat16 [16384, 2048], P(('ep', 'tp'))
Inputs may be any that keep to these rules, and one draw needn't show every extreme that they name: `routes`: each row names 2 different experts. In each aligned block of 256 rows no expert is named by more than 16 rows, and in some blocks an expert is named by exactly 16 rows.
All inputs are finite; a program needn't handle non-finite values.
Results may differ from a plain program's by a relative error of at most 0.012.
Values may be sent and summed in bfloat16 or wider, within the bound.
No kernel may reach another device: no remote copies, remote signals or barrier semaphores. Data moves between devices by JAX's collectives and lax.ppermute only.
A program may use at most 128 MiB of HBM per device.

v0:
```python
import jax
import jax.numpy as jnp
from jax import lax
from jax.experimental import pallas as pl
from jax.experimental.pallas import tpu as pltpu
from jax.sharding import PartitionSpec as P


def shifted(value, axis, steps):
    count = lax.axis_size(axis)
    leading, last = (max(0, -steps), min(count, count - steps))
    return lax.ppermute(value, axis, [(source, source + steps) for source in range(leading, last)])


def turned(value, steps):
    count = lax.axis_size("tp")
    return lax.ppermute(value, "tp", [(i, (i + steps) % count) for i in range(count)])


def dot(lhs, rhs):
    return jnp.dot(lhs, rhs, preferred_element_type=jnp.float32)


def in_three(value):
    high = lax.reduce_precision(value, 8, 7)
    rest = value - high
    middle = lax.reduce_precision(rest, 8, 7)
    low = rest - middle
    return [term.astype(jnp.bfloat16) for term in (high, middle, low)]


def tied(*values):
    return lax.optimization_barrier(values)


def rounded_sum(*values):
    return sum(value.astype(jnp.float32) for value in values).astype(jnp.bfloat16)


def expert_body(top_ref, low_ref, gate_ref, up_ref, down_ref, top_out, low_out, rows, total):
    step = pl.program_id(0)
    half = top_ref.shape[0]

    @pl.when(step == 0)
    def _():
        rows[:half] = top_ref[...]
        rows[half:] = low_ref[...]

    gated = dot(rows[...], gate_ref[0])
    raised = dot(rows[...], up_ref[0])
    hidden = (gated / (1.0 + jnp.exp(-gated)) * raised).astype(jnp.bfloat16)
    added = dot(hidden, down_ref[0])

    @pl.when(step == 0)
    def _():
        total[...] = added

    @pl.when(step == pl.num_programs(0) - 1)
    def _():
        top_out[...] = (total[:half] + added[:half]).astype(jnp.bfloat16)
        low_out[...] = (total[half:] + added[half:]).astype(jnp.bfloat16)


def expert(top, low, gate_proj, up_proj, down_proj):
    half, width = top.shape
    hidden = gate_proj.shape[2]
    steps = 2
    tile = hidden // steps
    block = pl.BlockSpec((half, width), lambda i: (0, 0))
    shape = jax.ShapeDtypeStruct((half, width), jnp.bfloat16)
    return pl.pallas_call(
        expert_body,
        grid=(steps,),
        in_specs=[
            block,
            block,
            pl.BlockSpec((1, width, tile), lambda i: (0, 0, i)),
            pl.BlockSpec((1, width, tile), lambda i: (0, 0, i)),
            pl.BlockSpec((1, tile, width), lambda i: (0, i, 0)),
        ],
        out_specs=[block, block],
        out_shape=[shape, shape],
        scratch_shapes=[
            pltpu.VMEM((2 * half, width), jnp.bfloat16),
            pltpu.VMEM((2 * half, width), jnp.float32),
        ],
        compiler_params=pltpu.CompilerParams(
            dimension_semantics=("arbitrary",), vmem_limit_bytes=32 * 1024 * 1024
        ),
        cost_estimate=pl.CostEstimate(
            flops=12 * half * width * hidden,
            bytes_accessed=6 * width * hidden + 8 * half * width,
            transcendentals=2 * half * hidden,
        ),
        name="expert",
    )(top, low, gate_proj, up_proj, down_proj)


def taps_body(rows_ref, history_ref, taps_ref, mixed_ref, sums_ref, squares_ref, window, taps):
    count, width = rows_ref.shape
    reach = taps_ref.shape[0] - 1
    lead = history_ref.shape[0]
    lanes = window.shape[2]
    tiles = width // lanes
    for tile in range(tiles):
        columns = slice(tile * lanes, (tile + 1) * lanes)
        window[tile, :lead] = history_ref[:, columns].astype(jnp.float32)
        window[tile, lead:] = rows_ref[:, columns].astype(jnp.float32)
        taps[tile, : reach + 1] = taps_ref[:, columns].astype(jnp.float32)
    block = 128
    ones = jnp.ones((8, lanes), jnp.float32)

    def across_lanes(value):
        return lax.dot_general(
            ones,
            value,
            (((1,), (1,)), ((), ())),
            precision=lax.Precision.HIGHEST,
            preferred_element_type=jnp.float32,
        )[0:1]

    @pl.loop(0, count // block)
    def _(step):
        base = step * block

        def one(tile, carry):
            total = jnp.zeros((block, lanes), jnp.float32)
            for offset in range(reach + 1):
                part = window[tile, pl.ds(base + (lead - reach + offset), block), :]
                total = total + part * taps[tile, offset : offset + 1, :]
            at = pl.multiple_of(base, block)
            mixed_ref[tile, pl.ds(at, block), :] = total
            return carry

        lax.fori_loop(0, tiles, one, 0)
        at = pl.multiple_of(base, block)
        parts = [mixed_ref[tile, pl.ds(at, block), :] for tile in range(tiles)]
        sums_ref[pl.ds(step, 1), :] = across_lanes(sum(parts))
        squares_ref[pl.ds(step, 1), :] = across_lanes(sum(part * part for part in parts))


def convolved(rows, history, taps):
    count, width = rows.shape
    lanes = 128
    tiles = width // lanes
    stats = jax.ShapeDtypeStruct((count // 128, 128), jnp.float32)
    return pl.pallas_call(
        taps_body,
        out_shape=[jax.ShapeDtypeStruct((tiles, count, lanes), jnp.float32), stats, stats],
        scratch_shapes=[
            pltpu.VMEM((tiles, count + history.shape[0], lanes), jnp.float32),
            pltpu.VMEM((tiles, 32, lanes), jnp.float32),
        ],
        compiler_params=pltpu.CompilerParams(vmem_limit_bytes=32 * 1024 * 1024),
        cost_estimate=pl.CostEstimate(
            flops=400 * taps.shape[0] * count * width,
            bytes_accessed=6 * count * width,
            transcendentals=0,
        ),
        name="taps",
    )(rows, history, taps)


def pick_body(select_ref, group_ref, out_ref):
    width = group_ref.shape[1]
    wide = 512
    for start in range(0, width, wide):
        columns = slice(start, start + wide)
        picked = dot(select_ref[...], group_ref[:, columns]).astype(jnp.bfloat16)
        out_ref[:, :, columns] = picked.reshape(out_ref.shape[0], out_ref.shape[1], wide)


def picked(select, group, share):
    slots, width = select.shape[0], group.shape[1]
    return pl.pallas_call(
        pick_body,
        out_shape=jax.ShapeDtypeStruct((slots // share, share, width), jnp.bfloat16),
        cost_estimate=pl.CostEstimate(
            flops=2 * slots * select.shape[1] * width,
            bytes_accessed=4 * slots * width,
            transcendentals=0,
        ),
        name="pick",
    )(select, group)


def halves_body(whole_ref, top_ref, low_ref):
    near = whole_ref.shape[0] // 2
    top_ref[...] = whole_ref[:near].reshape(top_ref.shape)
    low_ref[...] = whole_ref[near:].reshape(low_ref.shape)


def halves(whole):
    peers, share, width = whole.shape
    shape = jax.ShapeDtypeStruct((peers * share // 2, width), jnp.bfloat16)
    return pl.pallas_call(halves_body, out_shape=[shape, shape], name="halves")(whole)


def close_body(*refs):
    out_ref = refs[-1]
    near = out_ref.shape[0] // 2
    for index in range(2):
        terms = [ref[...].astype(jnp.float32) for ref in refs[3 * index : 3 * index + 3]]
        whole = (terms[0] + terms[1] + terms[2]).astype(jnp.bfloat16)
        out_ref[near * index : near * (index + 1)] = whole.reshape(near, *out_ref.shape[1:])


def closed(top, low, peers):
    rows, width = top[0].shape
    return pl.pallas_call(
        close_body,
        out_shape=jax.ShapeDtypeStruct((peers, 2 * rows // peers, width), jnp.bfloat16),
        name="close",
    )(*top, *low)


def mix_body(returned_ref, *refs):
    out_ref = refs[-1]
    slots = returned_ref.shape[0] * returned_ref.shape[1]
    width = returned_ref.shape[2]
    wide = 512
    for start in range(0, width, wide):
        columns = slice(start, start + wide)
        rows = returned_ref[:, :, columns].reshape(slots, wide)
        total = sum(
            lax.dot_general(
                ref[...], rows, (((0,), (0,)), ((), ())), preferred_element_type=jnp.float32
            )
            for ref in refs[:3]
        )
        out_ref[:, columns] = total.astype(jnp.bfloat16)


def mixed_in(returned, terms):
    width = returned.shape[2]
    return pl.pallas_call(
        mix_body,
        out_shape=jax.ShapeDtypeStruct((terms[0].shape[1], width), jnp.bfloat16),
        name="mix",
    )(returned, *terms)


def local(
    conv_input,
    conv_kernel,
    norm_gain,
    norm_shift,
    conv_proj,
    moe_input,
    moe_gain,
    routes,
    route_weights,
    gate_proj,
    up_proj,
    down_proj,
):
    tp_count = lax.axis_size("tp")
    ep_count = lax.axis_size("ep")
    tp_index = lax.axis_index("tp")
    group_rows, top_count = routes.shape
    own_rows, model_width = moe_input.shape
    capacity = 2 * top_count * group_rows // ep_count
    share = capacity // tp_count
    slots = ep_count * share

    moe_float = moe_input.astype(jnp.float32)
    normed = (
        moe_float
        * lax.rsqrt(jnp.mean(moe_float * moe_float, axis=1, keepdims=True) + 1e-06)
        * moe_gain
    ).astype(jnp.bfloat16)
    group = lax.all_to_all(
        jnp.broadcast_to(normed[None], (tp_count, own_rows, model_width)), "tp", 0, 0, tiled=True
    ).reshape(group_rows, model_width)

    experts = jnp.arange(ep_count, dtype=jnp.int32)
    hits = routes.T[:, None, :] == experts[None, :, None]
    chosen = jnp.any(hits, axis=0)
    before = (
        lax.broadcasted_iota(jnp.int32, (group_rows, group_rows), 0)
        < lax.broadcasted_iota(jnp.int32, (group_rows, group_rows), 1)
    ).astype(jnp.bfloat16)
    rank = dot(chosen.astype(jnp.bfloat16), before).astype(jnp.int32)
    local_rank = jnp.where(chosen, rank - tp_index * share, -1)
    select = local_rank[:, None, :] == jnp.arange(share, dtype=jnp.int32)[None, :, None]
    select = select.astype(jnp.bfloat16).reshape(slots, group_rows)

    local_rows, local_width = conv_input.shape
    history = shifted(conv_input[local_rows - 32 :], "ep", 1)
    mixed, *stats = convolved(conv_input, history, conv_kernel)
    group, select, mixed, *stats = tied(group, select, mixed, *stats)

    rows = picked(select, group, share)
    rows, routes, route_weights, *stats = tied(rows, routes, route_weights, *stats)
    landed = lax.all_to_all(rows, "ep", split_axis=0, concat_axis=0, tiled=True)

    hits = routes.T[:, None, :] == experts[None, :, None]
    weight_of = jnp.sum(jnp.where(hits, route_weights.T[:, None, :], 0.0), axis=0)
    weights = jnp.repeat(weight_of, share, axis=0) * select.astype(jnp.float32)
    terms = in_three(weights)

    full_width = local_width * tp_count
    sums, squares = lax.psum(tuple(stats), "tp")
    center = sums / full_width
    spread = jnp.maximum(squares / full_width - center * center, 0.0)
    factor = lax.rsqrt(spread + 1e-05)
    mixed = jnp.concatenate(list(mixed), axis=1)
    scaled = (mixed - center.reshape(-1, 1)) * factor.reshape(-1, 1) * norm_gain + norm_shift
    activated = jax.nn.silu(scaled).astype(jnp.bfloat16)
    half = local_rows // (2 * tp_count)

    def projected(step):
        start = lax.rem(tp_index + step, tp_count) * (2 * half)
        pair = []
        for offset in (0, half):
            part = lax.dynamic_slice_in_dim(activated, start + offset, half, axis=0)
            pair.append(dot(part, conv_proj).astype(jnp.bfloat16))
        return pair

    conv_far = projected(2)
    conv_right = projected(1)
    conv_left = projected(3)
    conv_own = projected(0)
    via_left = turned(conv_far[0], 1)
    via_right = turned(conv_far[1], -1)
    conv_right[0] = rounded_sum(conv_right[0], via_left)
    conv_left[1] = rounded_sum(conv_left[1], via_right)
    landed, *terms = tied(landed, *terms)
    landed, *rest = tied(landed, *conv_right, *conv_left, *conv_own)
    conv_right, conv_left, conv_own = rest[:2], rest[2:4], rest[4:]

    own = halves(landed)
    left_top, right_low = turned(own[0], 1), turned(own[1], -1)
    left_low, right_top = turned(own[1], 1), turned(own[0], -1)
    matrices = (gate_proj, up_proj, down_proj)
    own = expert(*own, *matrices)
    left_top, right_low, *own = tied(left_top, right_low, *own)
    far_top, far_low = turned(left_top, 1), turned(right_low, -1)
    left_top, right_low = expert(left_top, right_low, *matrices)
    left_top, right_low, right_top, left_low = tied(left_top, right_low, right_top, left_low)
    early_left, early_right = turned(right_low, 1), turned(left_top, -1)
    right_top, left_low = expert(right_top, left_low, *matrices)
    far_top, far_low, right_top, left_low = tied(far_top, far_low, right_top, left_low)
    far_top, far_low = expert(far_top, far_low, *matrices)

    right_top = rounded_sum(right_top, turned(far_top, 1))
    left_low = rounded_sum(left_low, turned(far_low, -1))
    flat = tied(right_top, left_low, *conv_right, *conv_left)
    right_top, left_low, conv_right, conv_left = flat[0], flat[1], flat[2:4], flat[4:6]
    late_left, late_right = turned(right_top, 1), turned(left_low, -1)
    conv_top = [turned(conv_right[0], 1), turned(conv_left[0], -1)]
    conv_low = [turned(conv_right[1], 1), turned(conv_left[1], -1)]
    totals = closed((own[0], late_left, early_right), (own[1], early_left, late_right), ep_count)

    returned = lax.all_to_all(totals, "ep", split_axis=0, concat_axis=0, tiled=True)
    combined = mixed_in(returned, terms)
    conv_out = jnp.concatenate(
        [rounded_sum(conv_own[0], *conv_top), rounded_sum(conv_own[1], *conv_low)], axis=0
    )
    parts = lax.all_to_all(
        combined.reshape(tp_count, own_rows, model_width), "tp", 0, 0, tiled=True
    )
    parts, conv_out = tied(parts, conv_out)
    moe_out = jnp.sum(parts.astype(jnp.float32), axis=0).astype(jnp.bfloat16)
    return (conv_out, moe_out)


def solution(mesh):
    placed = (
        P("ep", "tp"),
        P(None, "tp"),
        P("tp"),
        P("tp"),
        P("tp", None),
        P(("ep", "tp"), None),
        P(),
        P("ep", None),
        P("ep", None),
        P("ep", None, "tp"),
        P("ep", None, "tp"),
        P("ep", "tp", None),
    )
    return jax.shard_map(
        local,
        mesh=mesh,
        in_specs=placed,
        out_specs=(P(("ep", "tp"), None), P(("ep", "tp"), None)),
        check_vma=False,
    )
```

profile of v0, /device:TPU:32, one launch (start us, length us, event | category | flops | bytes accessed | tf_op | source)
XLA Modules:
  0.0 220.3 jit_solution(1536006432619912240)
XLA Ops:
  1.6 2.0 collective-permute-start
  6.9 4.6 %all-to-all-start = ((bf16[4,64,2048]{2,1,0:T(8,128)(2,1)}), bf16[4,64,2048]{2,1,0:T(8,128)(2,1)}, u32[]{:S(2)}, u32[]{:S(2)}) async-start(bf16[4,64,2048]{2,1,0:T(8,128)(2,1)} %broadcast_in_dim.16), calls=%async_computation | async-start | bytes 2097152 | tf_op jit(solution)/shard_map/all_to_all | solution.py:272
  12.7 1.7 compare_convert_fusion.select_ref
  14.4 7.5 %taps.1 = (f32[4,1024,128]{2,1,0:T(8,128)S(1)}, f32[8,128]{1,0:T(8,128)S(1)}, f32[8,128]{1,0:T(8,128)S(1)}) custom-call(bf16[1024,512]{1,0:T(8,128)(2,1)S(1)} %copy-done.12, bf16[32,512]{1,0:T(8,128)(2,1)S(1)} %collective-permute-done.history_ref, bf16[31,512]{1,0:T(8,128)(2,1)S(1)} %copy-done.13), custom_call_target="tpu_custom_call" | custom-call | flops 6501171200 | bytes 3145728 | tf_op jit(solution)/shard_map/taps/pallas_call | solution.py:147
  21.9 1.4 copy-done.7
  23.3 4.5 %all-to-all-done = bf16[4,64,2048]{2,1,0:T(8,128)(2,1)} async-done(((bf16[4,64,2048]{2,1,0:T(8,128)(2,1)}), bf16[4,64,2048]{2,1,0:T(8,128)(2,1)}, u32[]{:S(2)}, u32[]{:S(2)}) %all-to-all-start) | async-done | bytes 1048608 | tf_op jit(solution)/shard_map/all_to_all | solution.py:272
  27.8 2.7 %pick.1 = bf16[64,4,2048]{2,1,0:T(4,128)(2,1)} custom-call(bf16[256,256]{1,0:T(8,128)(2,1)} %compare_convert_fusion.select_ref, bf16[256,2048]{1,0:T(8,128)(2,1)} %bitcast.group_ref), custom_call_target="tpu_custom_call" | custom-call | flops 268435456 | bytes 2097152 | tf_op jit(solution)/shard_map/pick/pallas_call | solution.py:175
  30.5 12.1 %all-to-all-start.1 = ((bf16[64,4,2048]{2,1,0:T(4,128)(2,1)}), bf16[64,4,2048]{2,1,0:T(4,128)(2,1)}, u32[]{:S(2)}, u32[]{:S(2)}) async-start(bf16[64,4,2048]{2,1,0:T(4,128)(2,1)} %pick.1), calls=%async_computation.1 | async-start | bytes 2097152 | tf_op jit(solution)/shard_map/all_to_all | solution.py:295
  42.6 2.9 %slice_bitcast_fusion.3 = (f32[1024,128]{1,0:T(8,128)}, f32[1024,128]{1,0:T(8,128)}, f32[1024,128]{1,0:T(8,128)}, f32[1024,128]{1,0:T(8,128)}) fusion(f32[4,1024,128]{2,1,0:T(8,128)} %copy-done.7), kind=kLoop, calls=%fused_computation.33 | loop fusion | bytes 4194304 | tf_op jit(solution)/shard_map/unstack | solution.py:307
  45.5 9.0 %all-reduce = (f32[8,128]{1,0:T(8,128)S(1)}, f32[8,128]{1,0:T(8,128)S(1)}) all-reduce(f32[8,128]{1,0:T(8,128)S(1)} %get-tuple-element.69, f32[8,128]{1,0:T(8,128)S(1)} %get-tuple-element.68), channel_id=1, replica_groups=mesh['ep'=64,'tp'=4] {'tp'}, use_global_device_ids=true, to_apply=%region_4.5 | all-reduce | flops 2048 | bytes 16384 | tf_op jit(solution)/shard_map/psum | solution.py:303
  54.5 2.2 %multiply_convert_fusion = bf16[1024,512]{1,0:T(8,128)(2,1)S(1)} fusion(f32[1024,128]{1,0:T(8,128)} %get-tuple-element.113, f32[1024,128]{1,0:T(8,128)} %get-tuple-element.114, f32[1024,128]{1,0:T(8,128)} %get-tuple-element.115, f32[1024,128]{1,0:T(8,128)} %get-tuple-element.112, f32[512]{0:T(512)S(1)} %copy-done.21, f32[512]{0:T(512)S(1)} %copy-done.22, ...), kind=kLoop, calls=%fused_computation.14 | loop fusion | flops 6291456 | bytes 3158016 | tf_op jit(solution)/shard_map/convert_element_type | solution.py:309
  56.8 1.3 convolution_convert_fusion.2
  58.0 1.3 convolution_convert_fusion.6
  62.0 2.4 %collective-permute-start.2 = (bf16[128,2048]{1,0:T(8,128)(2,1)}, bf16[128,2048]{1,0:T(8,128)(2,1)S(1)}, u32[]{:S(2)}, u32[]{:S(2)}) collective-permute-start(bf16[128,2048]{1,0:T(8,128)(2,1)} %convolution_convert_fusion.2), channel_id=1, source_target_pairs={{0,3},{1,0},{2,1},{3,2},{4,7},{5,4},{6,5},{7,6},{8,11},{9,8},{10,9... | collective-permute-start | bytes 1572872 | tf_op jit(solution)/shard_map/ppermute | solution.py:17
  64.4 1.2 convolution_convert_fusion
  66.9 1.2 convolution_convert_fusion.4
  68.1 1.2 convolution_convert_fusion.5
  70.2 5.1 %collective-permute-done.1 = bf16[128,2048]{1,0:T(8,128)(2,1)S(1)} collective-permute-done((bf16[128,2048]{1,0:T(8,128)(2,1)}, bf16[128,2048]{1,0:T(8,128)(2,1)S(1)}, u32[]{:S(2)}, u32[]{:S(2)}) %collective-permute-start.1) | collective-permute-done | bytes 524320 | tf_op jit(solution)/shard_map/ppermute | solution.py:17
  75.3 1.3 add_convert_fusion.5
  77.9 2.3 %halves.1 = (bf16[128,2048]{1,0:T(8,128)(2,1)}, bf16[128,2048]{1,0:T(8,128)(2,1)}) custom-call(bf16[64,4,2048]{2,1,0:T(4,128)(2,1)} %all-to-all-done.1.whole_ref), custom_call_target="tpu_custom_call" | custom-call | tf_op jit(solution)/shard_map/halves/pallas_call | solution.py:196
  80.1 3.2 %collective-permute-start.4 = (bf16[128,2048]{1,0:T(8,128)(2,1)}, bf16[128,2048]{1,0:T(8,128)(2,1)S(1)}, u32[]{:S(2)}, u32[]{:S(2)}) collective-permute-start(bf16[128,2048]{1,0:T(8,128)(2,1)} %get-tuple-element.72.low_ref), channel_id=1, source_target_pairs={{0,3},{1,0},{2,1},{3,2},{4,7},{5,4},{6,5},{7,6},{8,11},{9,8},{10,9... | collective-permute-start | bytes 1572872 | tf_op jit(solution)/shard_map/ppermute | solution.py:17
  83.8 1.6 collective-permute-start.8
  85.4 1.6 copy-done.1
  87.0 1.6 copy-done.3
  88.6 1.6 copy-done.5
  92.2 2.8 %expert.4 = (bf16[128,2048]{1,0:T(8,128)(2,1)S(1)}, bf16[128,2048]{1,0:T(8,128)(2,1)S(1)}) custom-call(bf16[128,2048]{1,0:T(8,128)(2,1)S(1)} %copy-done.9, bf16[128,2048]{1,0:T(8,128)(2,1)S(1)} %copy-done.8, bf16[1,2048,512]{2,1,0:T(8,128)(2,1)S(1)} %copy-done.1, bf16[1,2048,512]{2,1,0:T(8,128)(2,1)S(1)} %copy-done.3, bf16[1,512,2048]{2,1,0:T(8,128)(2,1)S(1)} %copy-done.5), custom_call_target="tpu_custom_call" | custom-call | flops 1610612736 | bytes 8388608 | tf_op jit(solution)/shard_map/expert/pallas_call | solution.py:71
  96.3 3.2 %collective-permute-start.6 = (bf16[128,2048]{1,0:T(8,128)(2,1)S(1)}, bf16[128,2048]{1,0:T(8,128)(2,1)S(1)}, u32[]{:S(2)}, u32[]{:S(2)}) collective-permute-start(bf16[128,2048]{1,0:T(8,128)(2,1)S(1)} %collective-permute-done.4.low_ref), channel_id=1, source_target_pairs={{0,3},{1,0},{2,1},{3,2},{4,7},{5,4},{6,5},{7,6},{8,11},{9,8},{10,9... | collective-permute-start | bytes 1572872 | tf_op jit(solution)/shard_map/ppermute | solution.py:17
  99.6 2.9 %expert.5 = (bf16[128,2048]{1,0:T(8,128)(2,1)S(1)}, bf16[128,2048]{1,0:T(8,128)(2,1)S(1)}) custom-call(bf16[128,2048]{1,0:T(8,128)(2,1)S(1)} %collective-permute-done.3.top_ref, bf16[128,2048]{1,0:T(8,128)(2,1)S(1)} %collective-permute-done.4.low_ref, bf16[1,2048,512]{2,1,0:T(8,128)(2,1)S(1)} %copy-done.2, bf16[1,2048,512]{2,1,0:T(8,128)(2,1)S(1)} %copy-done.4, ...), custom_call_target="tpu_custom_call" | custom-call | flops 1610612736 | bytes 8388608 | tf_op jit(solution)/shard_map/expert/pallas_call | solution.py:71
  102.5 4.7 %collective-permute-done.7.top_ref = bf16[128,2048]{1,0:T(8,128)(2,1)S(1)} collective-permute-done((bf16[128,2048]{1,0:T(8,128)(2,1)}, bf16[128,2048]{1,0:T(8,128)(2,1)S(1)}, u32[]{:S(2)}, u32[]{:S(2)}) %collective-permute-start.7) | collective-permute-done | bytes 524320 | tf_op jit(solution)/shard_map/ppermute | solution.py:17
  107.6 2.9 %expert.6 = (bf16[128,2048]{1,0:T(8,128)(2,1)S(1)}, bf16[128,2048]{1,0:T(8,128)(2,1)S(1)}) custom-call(bf16[128,2048]{1,0:T(8,128)(2,1)S(1)} %collective-permute-done.7.top_ref, bf16[128,2048]{1,0:T(8,128)(2,1)S(1)} %collective-permute-done.8.low_ref, bf16[1,2048,512]{2,1,0:T(8,128)(2,1)S(1)} %copy-done.2, bf16[1,2048,512]{2,1,0:T(8,128)(2,1)S(1)} %copy-done.4, ...), custom_call_target="tpu_custom_call" | custom-call | flops 1610612736 | bytes 8388608 | tf_op jit(solution)/shard_map/expert/pallas_call | solution.py:71
  110.4 5.4 %collective-permute-done.5.top_ref = bf16[128,2048]{1,0:T(8,128)(2,1)S(1)} collective-permute-done((bf16[128,2048]{1,0:T(8,128)(2,1)S(1)}, bf16[128,2048]{1,0:T(8,128)(2,1)S(1)}, u32[]{:S(2)}, u32[]{:S(2)}) %collective-permute-start.5) | collective-permute-done | bytes 524320 | tf_op jit(solution)/shard_map/ppermute | solution.py:17
  115.9 2.9 %expert.7 = (bf16[128,2048]{1,0:T(8,128)(2,1)S(1)}, bf16[128,2048]{1,0:T(8,128)(2,1)S(1)}) custom-call(bf16[128,2048]{1,0:T(8,128)(2,1)S(1)} %collective-permute-done.5.top_ref, bf16[128,2048]{1,0:T(8,128)(2,1)S(1)} %collective-permute-done.6.low_ref, bf16[1,2048,512]{2,1,0:T(8,128)(2,1)S(1)} %copy-done.2, bf16[1,2048,512]{2,1,0:T(8,128)(2,1)S(1)} %copy-done.4, ...), custom_call_target="tpu_custom_call" | custom-call | flops 1610612736 | bytes 8388608 | tf_op jit(solution)/shard_map/expert/pallas_call | solution.py:71
  118.8 3.2 %collective-permute-start.10 = (bf16[128,2048]{1,0:T(8,128)(2,1)S(1)}, bf16[128,2048]{1,0:T(8,128)(2,1)S(1)}, u32[]{:S(2)}, u32[]{:S(2)}) collective-permute-start(bf16[128,2048]{1,0:T(8,128)(2,1)S(1)} %get-tuple-element.89), channel_id=1, source_target_pairs={{0,3},{1,0},{2,1},{3,2},{4,7},{5,4},{6,5},{7,6},{8,11},{9,8},{10,9... | collective-permute-start | bytes 1572872 | tf_op jit(solution)/shard_map/ppermute | solution.py:17
  122.1 1.7 collective-permute-start.12
  124.1 10.7 %collective-permute-done.9 = bf16[128,2048]{1,0:T(8,128)(2,1)S(1)} collective-permute-done((bf16[128,2048]{1,0:T(8,128)(2,1)S(1)}, bf16[128,2048]{1,0:T(8,128)(2,1)S(1)}, u32[]{:S(2)}, u32[]{:S(2)}) %collective-permute-start.9) | collective-permute-done | bytes 524320 | tf_op jit(solution)/shard_map/ppermute | solution.py:17
  136.2 2.4 %collective-permute-start.14 = (bf16[128,2048]{1,0:T(8,128)(2,1)S(1)}, bf16[128,2048]{1,0:T(8,128)(2,1)}, u32[]{:S(2)}, u32[]{:S(2)}) collective-permute-start(bf16[128,2048]{1,0:T(8,128)(2,1)S(1)} %add_convert_fusion.2), channel_id=1, source_target_pairs={{0,3},{1,0},{2,1},{3,2},{4,7},{5,4},{6,5},{7,6},{8,11},{9,8},{10,9... | collective-permute-start | bytes 1572872 | tf_op jit(solution)/shard_map/ppermute | solution.py:17
  138.6 7.0 %collective-permute-done.12.refs_2_ = bf16[128,2048]{1,0:T(8,128)(2,1)S(1)} collective-permute-done((bf16[128,2048]{1,0:T(8,128)(2,1)S(1)}, bf16[128,2048]{1,0:T(8,128)(2,1)S(1)}, u32[]{:S(2)}, u32[]{:S(2)}) %collective-permute-start.12) | collective-permute-done | bytes 524320 | tf_op jit(solution)/shard_map/ppermute | solution.py:17
  146.1 7.5 %collective-permute-done.11.refs_1_ = bf16[128,2048]{1,0:T(8,128)(2,1)S(1)} collective-permute-done((bf16[128,2048]{1,0:T(8,128)(2,1)S(1)}, bf16[128,2048]{1,0:T(8,128)(2,1)S(1)}, u32[]{:S(2)}, u32[]{:S(2)}) %collective-permute-start.11) | collective-permute-done | bytes 524320 | tf_op jit(solution)/shard_map/ppermute | solution.py:17
  154.3 3.2 %close.1 = bf16[64,4,2048]{2,1,0:T(4,128)(2,1)} custom-call(bf16[128,2048]{1,0:T(8,128)(2,1)} %copy-done.10, bf16[128,2048]{1,0:T(8,128)(2,1)} %copy-done.19, bf16[128,2048]{1,0:T(8,128)(2,1)} %copy-done.17, bf16[128,2048]{1,0:T(8,128)(2,1)} %copy-done.11, bf16[128,2048]{1,0:T(8,128)(2,1)} %copy-done.18, bf16[128,2048]{1,0:T(8,128)(2,1)} %collective-permute-done.14.refs_5_), custom_call_target="tpu_custom_call" | custom-call | tf_op jit(solution)/shard_map/close/pallas_call | solution.py:210
  157.6 10.3 %all-to-all-start.2 = ((bf16[64,4,2048]{2,1,0:T(4,128)(2,1)}), bf16[64,4,2048]{2,1,0:T(4,128)(2,1)S(1)}, u32[]{:S(2)}, u32[]{:S(2)}) async-start(bf16[64,4,2048]{2,1,0:T(4,128)(2,1)} %close.1), calls=%async_computation.2 | async-start | bytes 2097152 | tf_op jit(solution)/shard_map/all_to_all | solution.py:355
  168.1 3.1 %collective-permute-start.16 = (bf16[128,2048]{1,0:T(8,128)(2,1)}, bf16[128,2048]{1,0:T(8,128)(2,1)}, u32[]{:S(2)}, u32[]{:S(2)}) collective-permute-start(bf16[128,2048]{1,0:T(8,128)(2,1)} %convolution_convert_fusion.4), channel_id=1, source_target_pairs={{0,3},{1,0},{2,1},{3,2},{4,7},{5,4},{6,5},{7,6},{8,11},{9,8},{10,9... | collective-permute-start | bytes 1572872 | tf_op jit(solution)/shard_map/ppermute | solution.py:17
  171.2 3.2 %collective-permute-start.18 = (bf16[128,2048]{1,0:T(8,128)(2,1)}, bf16[128,2048]{1,0:T(8,128)(2,1)}, u32[]{:S(2)}, u32[]{:S(2)}) collective-permute-start(bf16[128,2048]{1,0:T(8,128)(2,1)} %add_convert_fusion.4), channel_id=1, source_target_pairs={{0,3},{1,0},{2,1},{3,2},{4,7},{5,4},{6,5},{7,6},{8,11},{9,8},{10,9... | collective-permute-start | bytes 1572872 | tf_op jit(solution)/shard_map/ppermute | solution.py:17
  174.4 21.4 %all-to-all-done.2.returned_ref = bf16[64,4,2048]{2,1,0:T(4,128)(2,1)S(1)} async-done(((bf16[64,4,2048]{2,1,0:T(4,128)(2,1)}), bf16[64,4,2048]{2,1,0:T(4,128)(2,1)S(1)}, u32[]{:S(2)}, u32[]{:S(2)}) %all-to-all-start.2) | async-done | bytes 1048608 | tf_op jit(solution)/shard_map/all_to_all | solution.py:355
  196.8 3.3 %mix.1 = bf16[256,2048]{1,0:T(8,128)(2,1)} custom-call(bf16[64,4,2048]{2,1,0:T(4,128)(2,1)} %copy-done.14, bf16[256,256]{1,0:T(8,128)(2,1)} %get-tuple-element.99.refs_0_, bf16[256,256]{1,0:T(8,128)(2,1)} %get-tuple-element.100.refs_1_, bf16[256,256]{1,0:T(8,128)(2,1)} %get-tuple-element.101.refs_2_), custom_call_target="tpu_custom_call" | custom-call | tf_op jit(solution)/shard_map/mix/pallas_call | solution.py:236
  200.1 3.5 %all-to-all-start.3 = ((bf16[4,64,2048]{2,1,0:T(8,128)(2,1)}), bf16[4,64,2048]{2,1,0:T(8,128)(2,1)S(1)}, u32[]{:S(2)}, u32[]{:S(2)}) async-start(bf16[4,64,2048]{2,1,0:T(8,128)(2,1)} %bitcast.26), calls=%async_computation.3 | async-start | bytes 2097152 | tf_op jit(solution)/shard_map/all_to_all | solution.py:360
  203.7 1.6 add_convert_fusion.1
  205.3 1.4 add_convert_fusion
  207.9 11.5 %all-to-all-done.3 = bf16[4,64,2048]{2,1,0:T(8,128)(2,1)S(1)} async-done(((bf16[4,64,2048]{2,1,0:T(8,128)(2,1)}), bf16[4,64,2048]{2,1,0:T(8,128)(2,1)S(1)}, u32[]{:S(2)}, u32[]{:S(2)}) %all-to-all-start.3) | async-done | bytes 1048608 | tf_op jit(solution)/shard_map/all_to_all | solution.py:360
  (89 shorter events, 21.8 us)
Async XLA Ops:
  0.6 56.1 %copy-start = (bf16[512,2048]{1,0:T(8,128)(2,1)S(1)}, bf16[512,2048]{1,0:T(8,128)(2,1)}, u32[]{:S(2)}) copy-start(bf16[512,2048]{1,0:T(8,128)(2,1)} %param.16) | copy-start | bytes 6291460
  1.6 10.0 %copy-start.20 = (s32[256,2]{0,1:T(2,128)S(1)}, s32[256,2]{0,1:T(2,128)}, u32[]{:S(2)}) copy-start(s32[256,2]{0,1:T(2,128)} %param.19) | copy-start | bytes 6148
  1.6 12.8 %collective-permute-start = (bf16[32,512]{1,0:T(8,128)(2,1)S(1)}, bf16[32,512]{1,0:T(8,128)(2,1)S(1)}, u32[]{:S(2)}, u32[]{:S(2)}) collective-permute-start(bf16[32,512]{1,0:T(8,128)(2,1)S(1)} %slice.3), channel_id=1, source_target_pairs={{0,4},{4,8},{8,12},{12,16},{16,20},{20,24},{24,28},{28,32},{32,36}... | collective-permute-start | bytes 98312 | tf_op jit(solution)/shard_map/ppermute | solution.py:12
  6.9 7.5 %copy-start.12 = (bf16[1024,512]{1,0:T(8,128)(2,1)S(1)}, bf16[1024,512]{1,0:T(8,128)(2,1)}, u32[]{:S(2)}) copy-start(bf16[1024,512]{1,0:T(8,128)(2,1)} %rows_ref.1) | copy-start | bytes 3145732
  6.9 7.5 %copy-start.13 = (bf16[31,512]{1,0:T(8,128)(2,1)S(1)}, bf16[31,512]{1,0:T(8,128)(2,1)}, u32[]{:S(2)}) copy-start(bf16[31,512]{1,0:T(8,128)(2,1)} %taps_ref.1) | copy-start | bytes 95236
  6.9 20.8 %all-to-all-start = ((bf16[4,64,2048]{2,1,0:T(8,128)(2,1)}), bf16[4,64,2048]{2,1,0:T(8,128)(2,1)}, u32[]{:S(2)}, u32[]{:S(2)}) async-start(bf16[4,64,2048]{2,1,0:T(8,128)(2,1)} %broadcast_in_dim.16), calls=%async_computation | async-start | bytes 2097152 | tf_op jit(solution)/shard_map/all_to_all | solution.py:272
  21.9 1.4 copy-start.7
  30.5 47.4 %all-to-all-start.1 = ((bf16[64,4,2048]{2,1,0:T(4,128)(2,1)}), bf16[64,4,2048]{2,1,0:T(4,128)(2,1)}, u32[]{:S(2)}, u32[]{:S(2)}) async-start(bf16[64,4,2048]{2,1,0:T(4,128)(2,1)} %pick.1), calls=%async_computation.1 | async-start | bytes 2097152 | tf_op jit(solution)/shard_map/all_to_all | solution.py:295
  42.6 11.9 %copy-start.21 = (f32[512]{0:T(512)S(1)}, f32[512]{0:T(512)}, u32[]{:S(2)}) copy-start(f32[512]{0:T(512)} %param.15) | copy-start | bytes 6148
  42.6 11.9 %copy-start.22 = (f32[512]{0:T(512)S(1)}, f32[512]{0:T(512)}, u32[]{:S(2)}) copy-start(f32[512]{0:T(512)} %param.14) | copy-start | bytes 6148
  56.8 2.5 %copy-start.23 = (f32[256,2]{0,1:T(2,128)S(1)}, f32[256,2]{0,1:T(2,128)}, u32[]{:S(2)}) copy-start(f32[256,2]{0,1:T(2,128)} %param.20) | copy-start | bytes 6148
  61.1 14.2 %collective-permute-start.1 = (bf16[128,2048]{1,0:T(8,128)(2,1)}, bf16[128,2048]{1,0:T(8,128)(2,1)S(1)}, u32[]{:S(2)}, u32[]{:S(2)}) collective-permute-start(bf16[128,2048]{1,0:T(8,128)(2,1)} %convolution_convert_fusion.6), channel_id=1, source_target_pairs={{0,1},{1,2},{2,3},{3,0},{4,5},{5,6},{6,7},{7,4},{8,9},{9,10},{10,1... | collective-permute-start | bytes 1572872 | tf_op jit(solution)/shard_map/ppermute | solution.py:17
  62.0 14.6 %collective-permute-start.2 = (bf16[128,2048]{1,0:T(8,128)(2,1)}, bf16[128,2048]{1,0:T(8,128)(2,1)S(1)}, u32[]{:S(2)}, u32[]{:S(2)}) collective-permute-start(bf16[128,2048]{1,0:T(8,128)(2,1)} %convolution_convert_fusion.2), channel_id=1, source_target_pairs={{0,3},{1,0},{2,1},{3,2},{4,7},{5,4},{6,5},{7,6},{8,11},{9,8},{10,9... | collective-permute-start | bytes 1572872 | tf_op jit(solution)/shard_map/ppermute | solution.py:17
  66.9 2.5 %copy-start.16 = (bf16[256,256]{1,0:T(8,128)(2,1)S(1)}, bf16[256,256]{1,0:T(8,128)(2,1)}, u32[]{:S(2)}) copy-start(bf16[256,256]{1,0:T(8,128)(2,1)} %compare_convert_fusion.select_ref) | copy-start | bytes 393220
  80.1 16.2 %collective-permute-start.3 = (bf16[128,2048]{1,0:T(8,128)(2,1)}, bf16[128,2048]{1,0:T(8,128)(2,1)S(1)}, u32[]{:S(2)}, u32[]{:S(2)}) collective-permute-start(bf16[128,2048]{1,0:T(8,128)(2,1)} %get-tuple-element.71.top_ref), channel_id=1, source_target_pairs={{0,1},{1,2},{2,3},{3,0},{4,5},{5,6},{6,7},{7,4},{8,9},{9,10},{10,1... | collective-permute-start | bytes 1572872 | tf_op jit(solution)/shard_map/ppermute | solution.py:17
  80.1 16.2 %collective-permute-start.4 = (bf16[128,2048]{1,0:T(8,128)(2,1)}, bf16[128,2048]{1,0:T(8,128)(2,1)S(1)}, u32[]{:S(2)}, u32[]{:S(2)}) collective-permute-start(bf16[128,2048]{1,0:T(8,128)(2,1)} %get-tuple-element.72.low_ref), channel_id=1, source_target_pairs={{0,3},{1,0},{2,1},{3,2},{4,7},{5,4},{6,5},{7,6},{8,11},{9,8},{10,9... | collective-permute-start | bytes 1572872 | tf_op jit(solution)/shard_map/ppermute | solution.py:17
  83.3 23.9 %collective-permute-start.7 = (bf16[128,2048]{1,0:T(8,128)(2,1)}, bf16[128,2048]{1,0:T(8,128)(2,1)S(1)}, u32[]{:S(2)}, u32[]{:S(2)}) collective-permute-start(bf16[128,2048]{1,0:T(8,128)(2,1)} %get-tuple-element.71.top_ref), channel_id=1, source_target_pairs={{0,3},{1,0},{2,1},{3,2},{4,7},{5,4},{6,5},{7,6},{8,11},{9,8},{10,9... | collective-permute-start | bytes 1572872 | tf_op jit(solution)/shard_map/ppermute | solution.py:17
  83.8 23.8 %collective-permute-start.8 = (bf16[128,2048]{1,0:T(8,128)(2,1)}, bf16[128,2048]{1,0:T(8,128)(2,1)S(1)}, u32[]{:S(2)}, u32[]{:S(2)}) collective-permute-start(bf16[128,2048]{1,0:T(8,128)(2,1)} %get-tuple-element.72.low_ref), channel_id=1, source_target_pairs={{0,1},{1,2},{2,3},{3,0},{4,5},{5,6},{6,7},{7,4},{8,9},{9,10},{10,1... | collective-permute-start | bytes 1572872 | tf_op jit(solution)/shard_map/ppermute | solution.py:17
  85.4 1.6 copy-start.1
  87.0 1.6 copy-start.3
  88.6 1.6 copy-start.5
  90.2 1.0 copy-start.8
  91.2 1.0 copy-start.9
  92.2 7.3 %copy-start.2 = (bf16[1,2048,512]{2,1,0:T(8,128)(2,1)S(1)}, bf16[1,2048,512]{2,1,0:T(8,128)(2,1)}, u32[]{:S(2)}) copy-start(bf16[1,2048,512]{2,1,0:T(8,128)(2,1)} %gate_ref.7) | copy-start | bytes 6291460
  92.2 7.3 %copy-start.4 = (bf16[1,2048,512]{2,1,0:T(8,128)(2,1)S(1)}, bf16[1,2048,512]{2,1,0:T(8,128)(2,1)}, u32[]{:S(2)}) copy-start(bf16[1,2048,512]{2,1,0:T(8,128)(2,1)} %up_ref.7) | copy-start | bytes 6291460
  92.2 7.3 %copy-start.6 = (bf16[1,512,2048]{2,1,0:T(8,128)(2,1)S(1)}, bf16[1,512,2048]{2,1,0:T(8,128)(2,1)}, u32[]{:S(2)}) copy-start(bf16[1,512,2048]{2,1,0:T(8,128)(2,1)} %down_ref.7) | copy-start | bytes 6291460
  95.1 7.4 %copy-start.10 = (bf16[128,2048]{1,0:T(8,128)(2,1)}, bf16[128,2048]{1,0:T(8,128)(2,1)S(1)}, u32[]{:S(2)}) copy-start(bf16[128,2048]{1,0:T(8,128)(2,1)S(1)} %get-tuple-element.75.refs_0_) | copy-start | bytes 1572868
  95.1 7.4 %copy-start.11 = (bf16[128,2048]{1,0:T(8,128)(2,1)}, bf16[128,2048]{1,0:T(8,128)(2,1)S(1)}, u32[]{:S(2)}) copy-start(bf16[128,2048]{1,0:T(8,128)(2,1)S(1)} %get-tuple-element.96.refs_3_) | copy-start | bytes 1572868
  96.3 19.5 %collective-permute-start.5 = (bf16[128,2048]{1,0:T(8,128)(2,1)S(1)}, bf16[128,2048]{1,0:T(8,128)(2,1)S(1)}, u32[]{:S(2)}, u32[]{:S(2)}) collective-permute-start(bf16[128,2048]{1,0:T(8,128)(2,1)S(1)} %collective-permute-done.3.top_ref), channel_id=1, source_target_pairs={{0,1},{1,2},{2,3},{3,0},{4,5},{5,6},{6,7},{7,4},{8,9},{9,10},{10,1... | collective-permute-start | bytes 1572872 | tf_op jit(solution)/shard_map/ppermute | solution.py:17
  96.3 19.5 %collective-permute-start.6 = (bf16[128,2048]{1,0:T(8,128)(2,1)S(1)}, bf16[128,2048]{1,0:T(8,128)(2,1)S(1)}, u32[]{:S(2)}, u32[]{:S(2)}) collective-permute-start(bf16[128,2048]{1,0:T(8,128)(2,1)S(1)} %collective-permute-done.4.low_ref), channel_id=1, source_target_pairs={{0,3},{1,0},{2,1},{3,2},{4,7},{5,4},{6,5},{7,6},{8,11},{9,8},{10,9... | collective-permute-start | bytes 1572872 | tf_op jit(solution)/shard_map/ppermute | solution.py:17
  118.8 16.1 %collective-permute-start.9 = (bf16[128,2048]{1,0:T(8,128)(2,1)S(1)}, bf16[128,2048]{1,0:T(8,128)(2,1)S(1)}, u32[]{:S(2)}, u32[]{:S(2)}) collective-permute-start(bf16[128,2048]{1,0:T(8,128)(2,1)S(1)} %get-tuple-element.87), channel_id=1, source_target_pairs={{0,1},{1,2},{2,3},{3,0},{4,5},{5,6},{6,7},{7,4},{8,9},{9,10},{10,1... | collective-permute-start | bytes 1572872 | tf_op jit(solution)/shard_map/ppermute | solution.py:17
  118.8 16.1 %collective-permute-start.10 = (bf16[128,2048]{1,0:T(8,128)(2,1)S(1)}, bf16[128,2048]{1,0:T(8,128)(2,1)S(1)}, u32[]{:S(2)}, u32[]{:S(2)}) collective-permute-start(bf16[128,2048]{1,0:T(8,128)(2,1)S(1)} %get-tuple-element.89), channel_id=1, source_target_pairs={{0,3},{1,0},{2,1},{3,2},{4,7},{5,4},{6,5},{7,6},{8,11},{9,8},{10,9... | collective-permute-start | bytes 1572872 | tf_op jit(solution)/shard_map/ppermute | solution.py:17
  122.1 23.5 %collective-permute-start.12 = (bf16[128,2048]{1,0:T(8,128)(2,1)S(1)}, bf16[128,2048]{1,0:T(8,128)(2,1)S(1)}, u32[]{:S(2)}, u32[]{:S(2)}) collective-permute-start(bf16[128,2048]{1,0:T(8,128)(2,1)S(1)} %get-tuple-element.95), channel_id=1, source_target_pairs={{0,3},{1,0},{2,1},{3,2},{4,7},{5,4},{6,5},{7,6},{8,11},{9,8},{10,9... | collective-permute-start | bytes 1572872 | tf_op jit(solution)/shard_map/ppermute | solution.py:17
  123.8 22.3 %collective-permute-start.13 = (bf16[128,2048]{1,0:T(8,128)(2,1)S(1)}, bf16[128,2048]{1,0:T(8,128)(2,1)S(1)}, u32[]{:S(2)}, u32[]{:S(2)}) collective-permute-start(bf16[128,2048]{1,0:T(8,128)(2,1)S(1)} %get-tuple-element.97), channel_id=1, source_target_pairs={{0,1},{1,2},{2,3},{3,0},{4,5},{5,6},{6,7},{7,4},{8,9},{9,10},{10,1... | collective-permute-start | bytes 1572872 | tf_op jit(solution)/shard_map/ppermute | solution.py:17
  135.1 18.4 %collective-permute-start.11 = (bf16[128,2048]{1,0:T(8,128)(2,1)S(1)}, bf16[128,2048]{1,0:T(8,128)(2,1)S(1)}, u32[]{:S(2)}, u32[]{:S(2)}) collective-permute-start(bf16[128,2048]{1,0:T(8,128)(2,1)S(1)} %add_convert_fusion.3), channel_id=1, source_target_pairs={{0,1},{1,2},{2,3},{3,0},{4,5},{5,6},{6,7},{7,4},{8,9},{9,10},{10,1... | collective-permute-start | bytes 1572872 | tf_op jit(solution)/shard_map/ppermute | solution.py:17
  136.2 18.1 %collective-permute-start.14 = (bf16[128,2048]{1,0:T(8,128)(2,1)S(1)}, bf16[128,2048]{1,0:T(8,128)(2,1)}, u32[]{:S(2)}, u32[]{:S(2)}) collective-permute-start(bf16[128,2048]{1,0:T(8,128)(2,1)S(1)} %add_convert_fusion.2), channel_id=1, source_target_pairs={{0,3},{1,0},{2,1},{3,2},{4,7},{5,4},{6,5},{7,6},{8,11},{9,8},{10,9... | collective-permute-start | bytes 1572872 | tf_op jit(solution)/shard_map/ppermute | solution.py:17
  145.6 8.7 %copy-start.17 = (bf16[128,2048]{1,0:T(8,128)(2,1)}, bf16[128,2048]{1,0:T(8,128)(2,1)S(1)}, u32[]{:S(2)}) copy-start(bf16[128,2048]{1,0:T(8,128)(2,1)S(1)} %collective-permute-done.12.refs_2_) | copy-start | bytes 1572868
  146.1 8.3 %copy-start.18 = (bf16[128,2048]{1,0:T(8,128)(2,1)}, bf16[128,2048]{1,0:T(8,128)(2,1)S(1)}, u32[]{:S(2)}) copy-start(bf16[128,2048]{1,0:T(8,128)(2,1)S(1)} %collective-permute-done.13.refs_4_) | copy-start | bytes 1572868
  153.5 0.8 copy-start.19
  157.6 38.2 %all-to-all-start.2 = ((bf16[64,4,2048]{2,1,0:T(4,128)(2,1)}), bf16[64,4,2048]{2,1,0:T(4,128)(2,1)S(1)}, u32[]{:S(2)}, u32[]{:S(2)}) async-start(bf16[64,4,2048]{2,1,0:T(4,128)(2,1)} %close.1), calls=%async_computation.2 | async-start | bytes 2097152 | tf_op jit(solution)/shard_map/all_to_all | solution.py:355
  167.9 35.8 %collective-permute-start.15 = (bf16[128,2048]{1,0:T(8,128)(2,1)}, bf16[128,2048]{1,0:T(8,128)(2,1)}, u32[]{:S(2)}, u32[]{:S(2)}) collective-permute-start(bf16[128,2048]{1,0:T(8,128)(2,1)} %add_convert_fusion.5), channel_id=1, source_target_pairs={{0,1},{1,2},{2,3},{3,0},{4,5},{5,6},{6,7},{7,4},{8,9},{9,10},{10,1... | collective-permute-start | bytes 1572872 | tf_op jit(solution)/shard_map/ppermute | solution.py:17
  168.1 35.5 %collective-permute-start.16 = (bf16[128,2048]{1,0:T(8,128)(2,1)}, bf16[128,2048]{1,0:T(8,128)(2,1)}, u32[]{:S(2)}, u32[]{:S(2)}) collective-permute-start(bf16[128,2048]{1,0:T(8,128)(2,1)} %convolution_convert_fusion.4), channel_id=1, source_target_pairs={{0,3},{1,0},{2,1},{3,2},{4,7},{5,4},{6,5},{7,6},{8,11},{9,8},{10,9... | collective-permute-start | bytes 1572872 | tf_op jit(solution)/shard_map/ppermute | solution.py:17
  171.2 34.1 %collective-permute-start.17 = (bf16[128,2048]{1,0:T(8,128)(2,1)}, bf16[128,2048]{1,0:T(8,128)(2,1)}, u32[]{:S(2)}, u32[]{:S(2)}) collective-permute-start(bf16[128,2048]{1,0:T(8,128)(2,1)} %convolution_convert_fusion.5), channel_id=1, source_target_pairs={{0,1},{1,2},{2,3},{3,0},{4,5},{5,6},{6,7},{7,4},{8,9},{9,10},{10,1... | collective-permute-start | bytes 1572872 | tf_op jit(solution)/shard_map/ppermute | solution.py:17
  171.2 34.1 %collective-permute-start.18 = (bf16[128,2048]{1,0:T(8,128)(2,1)}, bf16[128,2048]{1,0:T(8,128)(2,1)}, u32[]{:S(2)}, u32[]{:S(2)}) collective-permute-start(bf16[128,2048]{1,0:T(8,128)(2,1)} %add_convert_fusion.4), channel_id=1, source_target_pairs={{0,3},{1,0},{2,1},{3,2},{4,7},{5,4},{6,5},{7,6},{8,11},{9,8},{10,9... | collective-permute-start | bytes 1572872 | tf_op jit(solution)/shard_map/ppermute | solution.py:17
  195.8 1.0 copy-start.14
  200.1 19.3 %all-to-all-start.3 = ((bf16[4,64,2048]{2,1,0:T(8,128)(2,1)}), bf16[4,64,2048]{2,1,0:T(8,128)(2,1)S(1)}, u32[]{:S(2)}, u32[]{:S(2)}) async-start(bf16[4,64,2048]{2,1,0:T(8,128)(2,1)} %bitcast.26), calls=%async_computation.3 | async-start | bytes 2097152 | tf_op jit(solution)/shard_map/all_to_all | solution.py:360
  203.6 1.7 copy-start.15
where the time goes:
time: 221 us; the launch traced here: 220 us
  waiting for transfers between devices  79.9 us (36%)
  starting transfers between devices  59.7 us (27%)
  Pallas kernels  30.5 us (14%)
  local copies, waits for them, and re-layouts  17.7 us (8%)
  other arithmetic  12.3 us (6%)
  matrix products  10.2 us (5%)
  blocking collectives  8.99 us (4%)
    ppermute x18, waiting for transfers between devices, turned(): lax.ppermute(value, 'tp', [(i, (i + steps) % count) for i in range(count)])  42.6 us
    ppermute x18, starting transfers between devices, turned(): lax.ppermute(value, 'tp', [(i, (i + steps) % count) for i in range(count)])  27.2 us
    all_to_all x1, waiting for transfers between devices, local(): lax.all_to_all(totals, 'ep', split_axis=0, concat_axis=0, tiled=True)  21.4 us
    all_to_all x1, starting transfers between devices, local(): landed = lax.all_to_all(rows, 'ep', split_axis=0, concat_axis=0, tiled=True)  12.1 us
    all_to_all x1, waiting for transfers between devices, local(): lax.all_to_all(combined.reshape(tp_count, own_rows, model_width), 'tp', 0...  11.5 us
    pallas_call x4, Pallas kernels, expert(): pl.pallas_call(expert_body, grid=(steps,), in_specs=[block, block, pl.Blo...  11.4 us
    all_to_all x1, starting transfers between devices, local(): lax.all_to_all(totals, 'ep', split_axis=0, concat_axis=0, tiled=True)  10.3 us
    dot_general x9, matrix products, dot(): return jnp.dot(lhs, rhs, preferred_element_type=jnp.float32)  10.2 us
  transfers between devices with their start and end apart: 23, of which 12 were waited for; matrix products, arithmetic and copies ran while one was open for 13% of the time, Pallas kernels for 9%

commit v1 on v0

--- a/solution.py
+++ b/solution.py
@@ -85,7 +85,7 @@
             pltpu.VMEM((2 * half, width), jnp.float32),
         ],
         compiler_params=pltpu.CompilerParams(
-            dimension_semantics=("arbitrary",), vmem_limit_bytes=32 * 1024 * 1024
+            dimension_semantics=("arbitrary",), vmem_limit_bytes=20 * 1024 * 1024
         ),
         cost_estimate=pl.CostEstimate(
             flops=12 * half * width * hidden,
@@ -151,7 +151,7 @@
             pltpu.VMEM((tiles, count + history.shape[0], lanes), jnp.float32),
             pltpu.VMEM((tiles, 32, lanes), jnp.float32),
         ],
-        compiler_params=pltpu.CompilerParams(vmem_limit_bytes=32 * 1024 * 1024),
+        compiler_params=pltpu.CompilerParams(vmem_limit_bytes=12 * 1024 * 1024),
         cost_estimate=pl.CostEstimate(
             flops=400 * taps.shape[0] * count * width,
             bytes_accessed=6 * count * width,
@@ -161,27 +161,33 @@
     )(rows, history, taps)
 
 
-def pick_body(select_ref, group_ref, out_ref):
-    width = group_ref.shape[1]
+def pick_body(select_ref, *refs):
+    pieces, out_ref, group = refs[:-2], refs[-2], refs[-1]
+    own = pieces[0].shape[0]
+    for index, piece in enumerate(pieces):
+        group[index * own : (index + 1) * own] = piece[...]
+    width = group.shape[1]
     wide = 512
     for start in range(0, width, wide):
         columns = slice(start, start + wide)
-        picked = dot(select_ref[...], group_ref[:, columns]).astype(jnp.bfloat16)
-        out_ref[:, :, columns] = picked.reshape(out_ref.shape[0], out_ref.shape[1], wide)
-
-
-def picked(select, group, share):
-    slots, width = select.shape[0], group.shape[1]
+        rows = dot(select_ref[...], group[:, columns]).astype(jnp.bfloat16)
+        out_ref[:, :, columns] = rows.reshape(out_ref.shape[0], out_ref.shape[1], wide)
+
+
+def picked(select, pieces, share):
+    slots, width = select.shape[0], pieces[0].shape[1]
     return pl.pallas_call(
         pick_body,
         out_shape=jax.ShapeDtypeStruct((slots // share, share, width), jnp.bfloat16),
+        scratch_shapes=[pltpu.VMEM((select.shape[1], width), jnp.bfloat16)],
         cost_estimate=pl.CostEstimate(
             flops=2 * slots * select.shape[1] * width,
             bytes_accessed=4 * slots * width,
             transcendentals=0,
         ),
+        compiler_params=pltpu.CompilerParams(vmem_limit_bytes=10 * 1024 * 1024),
         name="pick",
-    )(select, group)
+    )(select, *pieces)
 
 
 def halves_body(whole_ref, top_ref, low_ref):
@@ -193,7 +199,7 @@
 def halves(whole):
     peers, share, width = whole.shape
     shape = jax.ShapeDtypeStruct((peers * share // 2, width), jnp.bfloat16)
-    return pl.pallas_call(halves_body, out_shape=[shape, shape], name="halves")(whole)
+    return pl.pallas_call(halves_body, out_shape=[shape, shape], compiler_params=pltpu.CompilerParams(vmem_limit_bytes=10 * 1024 * 1024), name="halves")(whole)
 
 
 def close_body(*refs):
@@ -210,14 +216,16 @@
     return pl.pallas_call(
         close_body,
         out_shape=jax.ShapeDtypeStruct((peers, 2 * rows // peers, width), jnp.bfloat16),
+        compiler_params=pltpu.CompilerParams(vmem_limit_bytes=10 * 1024 * 1024),
         name="close",
     )(*top, *low)
 
 
 def mix_body(returned_ref, *refs):
-    out_ref = refs[-1]
+    terms, outs = refs[:3], refs[3:]
     slots = returned_ref.shape[0] * returned_ref.shape[1]
     width = returned_ref.shape[2]
+    own = outs[0].shape[0]
     wide = 512
     for start in range(0, width, wide):
         columns = slice(start, start + wide)
@@ -226,18 +234,16 @@
             lax.dot_general(
                 ref[...], rows, (((0,), (0,)), ((), ())), preferred_element_type=jnp.float32
             )
-            for ref in refs[:3]
-        )
-        out_ref[:, columns] = total.astype(jnp.bfloat16)
-
-
-def mixed_in(returned, terms):
+            for ref in terms
+        ).astype(jnp.bfloat16)
+        for index, out in enumerate(outs):
+            out[:, columns] = total[index * own : (index + 1) * own]
+
+
+def mixed_in(returned, terms, pieces):
     width = returned.shape[2]
-    return pl.pallas_call(
-        mix_body,
-        out_shape=jax.ShapeDtypeStruct((terms[0].shape[1], width), jnp.bfloat16),
-        name="mix",
-    )(returned, *terms)
+    own = jax.ShapeDtypeStruct((terms[0].shape[1] // pieces, width), jnp.bfloat16)
+    return pl.pallas_call(mix_body, out_shape=[own] * pieces, compiler_params=pltpu.CompilerParams(vmem_limit_bytes=10 * 1024 * 1024), name="mix")(returned, *terms)
 
 
 def local(
@@ -258,7 +264,7 @@
     ep_count = lax.axis_size("ep")
     tp_index = lax.axis_index("tp")
     group_rows, top_count = routes.shape
-    own_rows, model_width = moe_input.shape
+    own_rows, _ = moe_input.shape
     capacity = 2 * top_count * group_rows // ep_count
     share = capacity // tp_count
     slots = ep_count * share
@@ -269,9 +275,9 @@
         * lax.rsqrt(jnp.mean(moe_float * moe_float, axis=1, keepdims=True) + 1e-06)
         * moe_gain
     ).astype(jnp.bfloat16)
-    group = lax.all_to_all(
-        jnp.broadcast_to(normed[None], (tp_count, own_rows, model_width)), "tp", 0, 0, tiled=True
-    ).reshape(group_rows, model_width)
+    normed, conv_input = tied(normed, conv_input)
+    pieces = (normed, turned(normed, -1), turned(normed, 2), turned(normed, 1))
+    history = shifted(conv_input[conv_input.shape[0] - 32 :], "ep", 1)
 
     experts = jnp.arange(ep_count, dtype=jnp.int32)
     hits = routes.T[:, None, :] == experts[None, :, None]
@@ -282,23 +288,22 @@
     ).astype(jnp.bfloat16)
     rank = dot(chosen.astype(jnp.bfloat16), before).astype(jnp.int32)
     local_rank = jnp.where(chosen, rank - tp_index * share, -1)
-    select = local_rank[:, None, :] == jnp.arange(share, dtype=jnp.int32)[None, :, None]
+
+    def from_here(table):
+        return lax.dynamic_slice_in_dim(
+            jnp.concatenate([table, table], axis=1), tp_index * own_rows, group_rows, axis=1
+        )
+
+    select = from_here(local_rank)[:, None, :] == jnp.arange(share, dtype=jnp.int32)[None, :, None]
     select = select.astype(jnp.bfloat16).reshape(slots, group_rows)
+    *pieces, select, history = tied(*pieces, select, history)
+
+    rows = picked(select, pieces, share)
+    rows, routes, route_weights, conv_input = tied(rows, routes, route_weights, conv_input)
+    landed = lax.all_to_all(rows, "ep", split_axis=0, concat_axis=0, tiled=True)
 
     local_rows, local_width = conv_input.shape
-    history = shifted(conv_input[local_rows - 32 :], "ep", 1)
     mixed, *stats = convolved(conv_input, history, conv_kernel)
-    group, select, mixed, *stats = tied(group, select, mixed, *stats)
-
-    rows = picked(select, group, share)
-    rows, routes, route_weights, *stats = tied(rows, routes, route_weights, *stats)
-    landed = lax.all_to_all(rows, "ep", split_axis=0, concat_axis=0, tiled=True)
-
-    hits = routes.T[:, None, :] == experts[None, :, None]
-    weight_of = jnp.sum(jnp.where(hits, route_weights.T[:, None, :], 0.0), axis=0)
-    weights = jnp.repeat(weight_of, share, axis=0) * select.astype(jnp.float32)
-    terms = in_three(weights)
-
     full_width = local_width * tp_count
     sums, squares = lax.psum(tuple(stats), "tp")
     center = sums / full_width
@@ -309,59 +314,63 @@
     activated = jax.nn.silu(scaled).astype(jnp.bfloat16)
     half = local_rows // (2 * tp_count)
 
-    def projected(step):
-        start = lax.rem(tp_index + step, tp_count) * (2 * half)
-        pair = []
-        for offset in (0, half):
-            part = lax.dynamic_slice_in_dim(activated, start + offset, half, axis=0)
-            pair.append(dot(part, conv_proj).astype(jnp.bfloat16))
-        return pair
-
-    conv_far = projected(2)
-    conv_right = projected(1)
-    conv_left = projected(3)
-    conv_own = projected(0)
-    via_left = turned(conv_far[0], 1)
-    via_right = turned(conv_far[1], -1)
-    conv_right[0] = rounded_sum(conv_right[0], via_left)
-    conv_left[1] = rounded_sum(conv_left[1], via_right)
-    landed, *terms = tied(landed, *terms)
-    landed, *rest = tied(landed, *conv_right, *conv_left, *conv_own)
-    conv_right, conv_left, conv_own = rest[:2], rest[2:4], rest[4:]
+    def projected(rows, step, offset):
+        start = lax.rem(tp_index + step, tp_count) * (2 * half) + offset
+        part = lax.dynamic_slice_in_dim(rows, start, half, axis=0)
+        return dot(part, conv_proj).astype(jnp.bfloat16)
+
+    conv_top, conv_low = projected(activated, 2, 0), projected(activated, 2, half)
+    conv_top, conv_low = turned(conv_top, 1), turned(conv_low, -1)
+    landed, activated, routes, route_weights = tied(landed, activated, routes, route_weights)
 
     own = halves(landed)
     left_top, right_low = turned(own[0], 1), turned(own[1], -1)
     left_low, right_top = turned(own[1], 1), turned(own[0], -1)
     matrices = (gate_proj, up_proj, down_proj)
-    own = expert(*own, *matrices)
-    left_top, right_low, *own = tied(left_top, right_low, *own)
+    own = list(expert(*own, *matrices))
+    left_top, right_low, own[0] = tied(left_top, right_low, own[0])
     far_top, far_low = turned(left_top, 1), turned(right_low, -1)
+
+    activated, routes, route_weights, left_top = tied(activated, routes, route_weights, left_top)
+    hits = routes.T[:, None, :] == experts[None, :, None]
+    weight_of = jnp.sum(jnp.where(hits, route_weights.T[:, None, :], 0.0), axis=0)
+    weights = jnp.repeat(from_here(weight_of), share, axis=0) * select.astype(jnp.float32)
+    terms = in_three(weights)
+    conv_right = [projected(activated, 1, offset) for offset in (0, half)]
+    conv_left = [projected(activated, 3, offset) for offset in (0, half)]
+    conv_own = [projected(activated, 0, offset) for offset in (0, half)]
+
     left_top, right_low = expert(left_top, right_low, *matrices)
-    left_top, right_low, right_top, left_low = tied(left_top, right_low, right_top, left_low)
+    flat = tied(left_top, right_low, right_top, left_low, *conv_right, *conv_left, *conv_own, *terms)
+    left_top, right_low, right_top, left_low = flat[:4]
+    conv_right, conv_left, conv_own, terms = flat[4:6], flat[6:8], flat[8:10], flat[10:]
     early_left, early_right = turned(right_low, 1), turned(left_top, -1)
     right_top, left_low = expert(right_top, left_low, *matrices)
     far_top, far_low, right_top, left_low = tied(far_top, far_low, right_top, left_low)
     far_top, far_low = expert(far_top, far_low, *matrices)
-
-    right_top = rounded_sum(right_top, turned(far_top, 1))
-    left_low = rounded_sum(left_low, turned(far_low, -1))
-    flat = tied(right_top, left_low, *conv_right, *conv_left)
-    right_top, left_low, conv_right, conv_left = flat[0], flat[1], flat[2:4], flat[4:6]
-    late_left, late_right = turned(right_top, 1), turned(left_low, -1)
+    via_left, via_right = turned(far_top, 1), turned(far_low, -1)
+    conv_right = (rounded_sum(conv_right[0], conv_top), conv_right[1])
+    conv_left = (conv_left[0], rounded_sum(conv_left[1], conv_low))
+    via_left, via_right, *conv_sums = tied(via_left, via_right, conv_right[0], conv_left[1])
+    conv_right, conv_left = (conv_sums[0], conv_right[1]), (conv_left[0], conv_sums[1])
+    late_left = turned(rounded_sum(right_top, via_left), 1)
+    late_right = turned(rounded_sum(left_low, via_right), -1)
+    totals = closed(
+        (own[0], late_left, early_right), (own[1], early_left, late_right), ep_count
+    )
+
+    flat = tied(totals, *conv_right, *conv_left)
+    totals, conv_right, conv_left = flat[0], flat[1:3], flat[3:5]
+    returned = lax.all_to_all(totals, "ep", split_axis=0, concat_axis=0, tiled=True)
     conv_top = [turned(conv_right[0], 1), turned(conv_left[0], -1)]
     conv_low = [turned(conv_right[1], 1), turned(conv_left[1], -1)]
-    totals = closed((own[0], late_left, early_right), (own[1], early_left, late_right), ep_count)
-
-    returned = lax.all_to_all(totals, "ep", split_axis=0, concat_axis=0, tiled=True)
-    combined = mixed_in(returned, terms)
+    own, right, far, left = mixed_in(returned, terms, tp_count)
+    arrived = [turned(far, 2), turned(right, 1), turned(left, -1)]
     conv_out = jnp.concatenate(
         [rounded_sum(conv_own[0], *conv_top), rounded_sum(conv_own[1], *conv_low)], axis=0
     )
-    parts = lax.all_to_all(
-        combined.reshape(tp_count, own_rows, model_width), "tp", 0, 0, tiled=True
-    )
-    parts, conv_out = tied(parts, conv_out)
-    moe_out = jnp.sum(parts.astype(jnp.float32), axis=0).astype(jnp.bfloat16)
+    *arrived, conv_out = tied(*arrived, conv_out)
+    moe_out = rounded_sum(own, *arrived)
     return (conv_out, moe_out)
 
 

time: 221 us -> 206 us (0.932)
  waiting for transfers between devices: 79.9 us -> 69.8 us
  Pallas kernels: 30.5 us -> 25 us
  starting transfers between devices: 59.7 us -> 54.8 us
  other arithmetic: 12.3 us -> 15.7 us
  local copies, waits for them, and re-layouts: 17.7 us -> 15.2 us
    all_to_all x2 -> x0, waiting for transfers between devices: 16 us -> none  [the longest x1 11.5 us: local(): lax.all_to_all(combined.reshape(tp_count, own_rows, model_width), 'tp', 0...]
    ppermute x18 -> x24, waiting for transfers between devices: 42.6 us -> 55.4 us  [turned(): lax.ppermute(value, 'tp', [(i, (i + steps) % count) for i in range(count)])]
    all_to_all x1, waiting for transfers between devices: 21.4 us -> 9.52 us  [local(): lax.all_to_all(totals, 'ep', split_axis=0, concat_axis=0, tiled=True)]
    all_to_all x2 -> x0, starting transfers between devices: 8.12 us -> none  [the longest x1 4.59 us: local(): lax.all_to_all(jnp.broadcast_to(normed[None], (tp_count, own_rows, model_...]
    ppermute x18 -> x24, starting transfers between devices: 27.2 us -> 34.8 us  [turned(): lax.ppermute(value, 'tp', [(i, (i + steps) % count) for i in range(count)])]
    convert_element_type x4 -> x7, other arithmetic: 3.34 us -> 7.65 us  [rounded_sum(): sum((value.astype(jnp.float32) for value in values)).astype(jnp.bfloat16)]
    all_to_all x1, waiting for transfers between devices: 0.01 us -> 4.15 us  [local(): landed = lax.all_to_all(rows, 'ep', split_axis=0, concat_axis=0, tiled=True)]
    all_to_all x1, starting transfers between devices: 10.3 us -> 6.49 us  [local(): lax.all_to_all(totals, 'ep', split_axis=0, concat_axis=0, tiled=True)]
  transfers between devices with their start and end apart: 23 -> 27, of which waited for: 12 -> 13; matrix products, arithmetic and copies ran while one was open for 13% -> 15% of each run, Pallas kernels for 9% -> 11%
where the time goes in v1:
time: 206 us; the launch traced here: 204 us
  waiting for transfers between devices  69.8 us (34%)
  starting transfers between devices  54.8 us (27%)
  Pallas kernels  25 us (12%)
  other arithmetic  15.7 us (8%)
  local copies, waits for them, and re-layouts  15.2 us (7%)
  matrix products  12 us (6%)
  blocking collectives  9.98 us (5%)
    ppermute x24, waiting for transfers between devices, turned(): lax.ppermute(value, 'tp', [(i, (i + steps) % count) for i in range(count)])  55.4 us
    ppermute x24, starting transfers between devices, turned(): lax.ppermute(value, 'tp', [(i, (i + steps) % count) for i in range(count)])  34.8 us
    pallas_call x4, Pallas kernels, expert(): pl.pallas_call(expert_body, grid=(steps,), in_specs=[block, block, pl.Blo...  14.5 us
    dot_general x9, matrix products, dot(): return jnp.dot(lhs, rhs, preferred_element_type=jnp.float32)  12 us
    all_to_all x1, starting transfers between devices, local(): landed = lax.all_to_all(rows, 'ep', split_axis=0, concat_axis=0, tiled=True)  11.6 us
    psum x1, blocking collectives, local(): sums, squares = lax.psum(tuple(stats), 'tp')  9.98 us
    all_to_all x1, waiting for transfers between devices, local(): lax.all_to_all(totals, 'ep', split_axis=0, concat_axis=0, tiled=True)  9.52 us
    unnamed x54, local copies, waits for them, and re-layouts  9.37 us
  transfers between devices with their start and end apart: 27, of which 13 were waited for; matrix products, arithmetic and copies ran while one was open for 15% of the time, Pallas kernels for 11%

profile of v1, /device:TPU:32, one launch (start us, length us, event | category | flops | bytes accessed | tf_op | source)
XLA Modules:
  0.0 203.5 jit_solution(10669525061666271728)
XLA Ops:
  3.0 1.7 collective-permute-start.2
  4.7 2.9 %collective-permute-start.1 = (bf16[64,2048]{1,0:T(8,128)(2,1)S(1)}, bf16[64,2048]{1,0:T(8,128)(2,1)S(1)}, u32[]{:S(2)}, u32[]{:S(2)}) collective-permute-start(bf16[64,2048]{1,0:T(8,128)(2,1)S(1)} %fusion.7.refs_0_), channel_id=1, source_target_pairs={{0,2},{1,3},{2,0},{3,1},{4,6},{5,7},{6,4},{7,5},{8,10},{9,11},{10,... | collective-permute-start | bytes 786440 | tf_op jit(solution)/shard_map/ppermute | solution.py:17
  7.6 1.3 collective-permute-start
  9.7 1.9 collective-permute-start.3
  13.5 1.7 eq.50
  17.0 2.2 %collective-permute-done.1.refs_2_ = bf16[64,2048]{1,0:T(8,128)(2,1)S(1)} collective-permute-done((bf16[64,2048]{1,0:T(8,128)(2,1)S(1)}, bf16[64,2048]{1,0:T(8,128)(2,1)S(1)}, u32[]{:S(2)}, u32[]{:S(2)}) %collective-permute-start.1) | collective-permute-done | bytes 262176 | tf_op jit(solution)/shard_map/ppermute | solution.py:17
  20.6 11.6 %all-to-all-start = ((bf16[64,4,2048]{2,1,0:T(4,128)(2,1)}), bf16[64,4,2048]{2,1,0:T(4,128)(2,1)S(1)}, u32[]{:S(2)}, u32[]{:S(2)}) async-start(bf16[64,4,2048]{2,1,0:T(4,128)(2,1)} %copy-done.7), calls=%async_computation | async-start | bytes 2097152 | tf_op jit(solution)/shard_map/all_to_all | solution.py:303
  33.5 7.5 %taps.1 = (f32[4,1024,128]{2,1,0:T(8,128)S(1)}, f32[8,128]{1,0:T(8,128)S(1)}, f32[8,128]{1,0:T(8,128)S(1)}) custom-call(bf16[1024,512]{1,0:T(8,128)(2,1)S(1)} %copy-done.15, bf16[32,512]{1,0:T(8,128)(2,1)S(1)} %collective-permute-done.3.history_ref, bf16[31,512]{1,0:T(8,128)(2,1)S(1)} %copy-done.16), custom_call_target="tpu_custom_call" | custom-call | flops 6501171200 | bytes 3145728 | tf_op jit(solution)/shard_map/taps/pallas_call | solution.py:147
  41.0 1.4 copy-done.9
  42.4 10.0 %all-reduce = (f32[8,128]{1,0:T(8,128)S(1)}, f32[8,128]{1,0:T(8,128)S(1)}) all-reduce(f32[8,128]{1,0:T(8,128)S(1)} %get-tuple-element.84, f32[8,128]{1,0:T(8,128)S(1)} %get-tuple-element.83), channel_id=1, replica_groups=mesh['ep'=64,'tp'=4] {'tp'}, use_global_device_ids=true, to_apply=%region_3.4 | all-reduce | flops 2048 | bytes 16384 | tf_op jit(solution)/shard_map/psum | solution.py:308
  52.4 1.7 slice_bitcast_fusion.3
  54.1 1.9 multiply_convert_fusion
  56.0 4.1 %all-to-all-done.whole_ref = bf16[64,4,2048]{2,1,0:T(4,128)(2,1)S(1)} async-done(((bf16[64,4,2048]{2,1,0:T(4,128)(2,1)}), bf16[64,4,2048]{2,1,0:T(4,128)(2,1)S(1)}, u32[]{:S(2)}, u32[]{:S(2)}) %all-to-all-start) | async-done | bytes 1048608 | tf_op jit(solution)/shard_map/all_to_all | solution.py:303
  62.4 2.0 collective-permute-start.5
  64.4 2.1 %convolution_convert_fusion = bf16[128,2048]{1,0:T(8,128)(2,1)} fusion(bf16[512,2048]{1,0:T(8,128)(2,1)S(1)} %copy-done, bf16[1024,512]{1,0:T(8,128)(2,1)} %multiply_convert_fusion, s32[]{:T(128)S(6)} %select_n.46), kind=kOutput, calls=%fused_computation | convolution fusion | flops 268697600 | bytes 2752516 | tf_op jit(solution)/shard_map/dot_general | solution.py:21
  67.8 2.1 %convolution_convert_fusion.1 = bf16[128,2048]{1,0:T(8,128)(2,1)} fusion(bf16[512,2048]{1,0:T(8,128)(2,1)S(1)} %copy-done, bf16[1024,512]{1,0:T(8,128)(2,1)} %multiply_convert_fusion, s32[]{:T(128)S(6)} %select_n.45), kind=kOutput, calls=%fused_computation.1 | convolution fusion | flops 268697600 | bytes 2752516 | tf_op jit(solution)/shard_map/dot_general | solution.py:21
  72.0 3.9 %expert.4 = (bf16[128,2048]{1,0:T(8,128)(2,1)S(1)}, bf16[128,2048]{1,0:T(8,128)(2,1)S(1)}) custom-call(bf16[128,2048]{1,0:T(8,128)(2,1)} %get-tuple-element.88.top_ref, bf16[128,2048]{1,0:T(8,128)(2,1)} %get-tuple-element.89.low_ref, bf16[1,2048,512]{2,1,0:T(8,128)(2,1)S(1)} %copy-done.1, bf16[1,2048,512]{2,1,0:T(8,128)(2,1)S(1)} %copy-done.3, ...), custom_call_target="tpu_custom_call" | custom-call | flops 1610612736 | bytes 8388608 | tf_op jit(solution)/shard_map/expert/pallas_call | solution.py:71
  76.0 1.4 collective-permute-done.4.top_ref
  77.4 1.3 collective-permute-start.6
  85.0 1.3 convolution_convert_fusion.7
  87.3 1.9 collective-permute-start.7
  89.2 1.6 copy-done.2
  90.8 1.6 copy-done.4
  92.4 1.6 copy-done.6
  94.0 2.9 %expert.5 = (bf16[128,2048]{1,0:T(8,128)(2,1)S(1)}, bf16[128,2048]{1,0:T(8,128)(2,1)S(1)}) custom-call(bf16[128,2048]{1,0:T(8,128)(2,1)S(1)} %collective-permute-done.4.top_ref, bf16[128,2048]{1,0:T(8,128)(2,1)S(1)} %collective-permute-done.5.low_ref, bf16[1,2048,512]{2,1,0:T(8,128)(2,1)S(1)} %copy-done.2, bf16[1,2048,512]{2,1,0:T(8,128)(2,1)S(1)} %copy-done.4, ...), custom_call_target="tpu_custom_call" | custom-call | flops 1610612736 | bytes 8388608 | tf_op jit(solution)/shard_map/expert/pallas_call | solution.py:71
  97.6 2.4 %collective-permute-done.8.top_ref = bf16[128,2048]{1,0:T(8,128)(2,1)} collective-permute-done((bf16[128,2048]{1,0:T(8,128)(2,1)}, bf16[128,2048]{1,0:T(8,128)(2,1)}, u32[]{:S(2)}, u32[]{:S(2)}) %collective-permute-start.8) | collective-permute-done | bytes 524320 | tf_op jit(solution)/shard_map/ppermute | solution.py:17
  100.0 1.3 collective-permute-start.12
  101.3 2.0 collective-permute-start.15
  103.3 3.9 %expert.6 = (bf16[128,2048]{1,0:T(8,128)(2,1)S(1)}, bf16[128,2048]{1,0:T(8,128)(2,1)S(1)}) custom-call(bf16[128,2048]{1,0:T(8,128)(2,1)} %collective-permute-done.8.top_ref, bf16[128,2048]{1,0:T(8,128)(2,1)} %collective-permute-done.9.low_ref, bf16[1,2048,512]{2,1,0:T(8,128)(2,1)S(1)} %copy-done.2, bf16[1,2048,512]{2,1,0:T(8,128)(2,1)S(1)} %copy-done.4, ...), custom_call_target="tpu_custom_call" | custom-call | flops 1610612736 | bytes 8388608 | tf_op jit(solution)/shard_map/expert/pallas_call | solution.py:71
  107.4 3.8 %collective-permute-done.7.low_ref = bf16[128,2048]{1,0:T(8,128)(2,1)S(1)} collective-permute-done((bf16[128,2048]{1,0:T(8,128)(2,1)S(1)}, bf16[128,2048]{1,0:T(8,128)(2,1)S(1)}, u32[]{:S(2)}, u32[]{:S(2)}) %collective-permute-start.7) | collective-permute-done | bytes 524320 | tf_op jit(solution)/shard_map/ppermute | solution.py:17
  111.2 3.8 %expert.7 = (bf16[128,2048]{1,0:T(8,128)(2,1)S(1)}, bf16[128,2048]{1,0:T(8,128)(2,1)S(1)}) custom-call(bf16[128,2048]{1,0:T(8,128)(2,1)} %collective-permute-done.6.top_ref, bf16[128,2048]{1,0:T(8,128)(2,1)S(1)} %collective-permute-done.7.low_ref, bf16[1,2048,512]{2,1,0:T(8,128)(2,1)S(1)} %copy-done.2, bf16[1,2048,512]{2,1,0:T(8,128)(2,1)S(1)} %copy-done.4, ...), custom_call_target="tpu_custom_call" | custom-call | flops 1610612736 | bytes 8388608 | tf_op jit(solution)/shard_map/expert/pallas_call | solution.py:71
  115.0 1.4 collective-permute-start.10
  116.4 2.0 collective-permute-start.11
  118.4 2.0 add_convert_fusion.4
  121.3 14.6 %collective-permute-done.10 = bf16[128,2048]{1,0:T(8,128)(2,1)S(1)} collective-permute-done((bf16[128,2048]{1,0:T(8,128)(2,1)S(1)}, bf16[128,2048]{1,0:T(8,128)(2,1)S(1)}, u32[]{:S(2)}, u32[]{:S(2)}) %collective-permute-start.10) | collective-permute-done | bytes 524320 | tf_op jit(solution)/shard_map/ppermute | solution.py:17
  136.0 2.0 %collective-permute-start.17 = (bf16[128,2048]{1,0:T(8,128)(2,1)S(1)}, bf16[128,2048]{1,0:T(8,128)(2,1)S(1)}, u32[]{:S(2)}, u32[]{:S(2)}) collective-permute-start(bf16[128,2048]{1,0:T(8,128)(2,1)S(1)} %add_convert_fusion.2), channel_id=1, source_target_pairs={{0,3},{1,0},{2,1},{3,2},{4,7},{5,4},{6,5},{7,6},{8,11},{9,8},{10,9... | collective-permute-start | bytes 1572872 | tf_op jit(solution)/shard_map/ppermute | solution.py:17
  138.6 9.1 %collective-permute-done.17.refs_5_ = bf16[128,2048]{1,0:T(8,128)(2,1)S(1)} collective-permute-done((bf16[128,2048]{1,0:T(8,128)(2,1)S(1)}, bf16[128,2048]{1,0:T(8,128)(2,1)S(1)}, u32[]{:S(2)}, u32[]{:S(2)}) %collective-permute-start.17) | collective-permute-done | bytes 524320 | tf_op jit(solution)/shard_map/ppermute | solution.py:17
  147.7 2.7 %collective-permute-done.14.refs_1_ = bf16[128,2048]{1,0:T(8,128)(2,1)S(1)} collective-permute-done((bf16[128,2048]{1,0:T(8,128)(2,1)S(1)}, bf16[128,2048]{1,0:T(8,128)(2,1)S(1)}, u32[]{:S(2)}, u32[]{:S(2)}) %collective-permute-start.14) | collective-permute-done | bytes 524320 | tf_op jit(solution)/shard_map/ppermute | solution.py:17
  151.8 6.5 %all-to-all-start.1 = ((bf16[64,4,2048]{2,1,0:T(4,128)(2,1)}), bf16[64,4,2048]{2,1,0:T(4,128)(2,1)S(1)}, u32[]{:S(2)}, u32[]{:S(2)}) async-start(bf16[64,4,2048]{2,1,0:T(4,128)(2,1)} %copy-done.8), calls=%async_computation.1 | async-start | bytes 2097152 | tf_op jit(solution)/shard_map/all_to_all | solution.py:364
  158.4 3.2 %collective-permute-start.22 = (bf16[128,2048]{1,0:T(8,128)(2,1)}, bf16[128,2048]{1,0:T(8,128)(2,1)S(1)}, u32[]{:S(2)}, u32[]{:S(2)}) collective-permute-start(bf16[128,2048]{1,0:T(8,128)(2,1)} %convolution_convert_fusion.5), channel_id=1, source_target_pairs={{0,3},{1,0},{2,1},{3,2},{4,7},{5,4},{6,5},{7,6},{8,11},{9,8},{10,9... | collective-permute-start | bytes 1572872 | tf_op jit(solution)/shard_map/ppermute | solution.py:17
  161.6 3.2 %collective-permute-start.24 = (bf16[128,2048]{1,0:T(8,128)(2,1)}, bf16[128,2048]{1,0:T(8,128)(2,1)}, u32[]{:S(2)}, u32[]{:S(2)}) collective-permute-start(bf16[128,2048]{1,0:T(8,128)(2,1)} %add_convert_fusion.4), channel_id=1, source_target_pairs={{0,3},{1,0},{2,1},{3,2},{4,7},{5,4},{6,5},{7,6},{8,11},{9,8},{10,9... | collective-permute-start | bytes 1572872 | tf_op jit(solution)/shard_map/ppermute | solution.py:17
  164.8 9.7 %collective-permute-done.21 = bf16[128,2048]{1,0:T(8,128)(2,1)S(1)} collective-permute-done((bf16[128,2048]{1,0:T(8,128)(2,1)}, bf16[128,2048]{1,0:T(8,128)(2,1)S(1)}, u32[]{:S(2)}, u32[]{:S(2)}) %collective-permute-start.21) | collective-permute-done | bytes 524320 | tf_op jit(solution)/shard_map/ppermute | solution.py:17
  174.6 2.1 %add_convert_fusion.1 = bf16[128,2048]{1,0:T(8,128)(2,1)} fusion(bf16[128,2048]{1,0:T(8,128)(2,1)S(1)} %collective-permute-done.22, bf16[128,2048]{1,0:T(8,128)(2,1)S(1)} %collective-permute-done.21, bf16[128,2048]{1,0:T(8,128)(2,1)} %convolution_convert_fusion.3), kind=kLoop, calls=%fused_computation.18 | loop fusion | flops 1572864 | bytes 2097152 | tf_op jit(solution)/shard_map/convert_element_type | solution.py:37
  176.7 9.5 %all-to-all-done.1.returned_ref = bf16[64,4,2048]{2,1,0:T(4,128)(2,1)S(1)} async-done(((bf16[64,4,2048]{2,1,0:T(4,128)(2,1)}), bf16[64,4,2048]{2,1,0:T(4,128)(2,1)S(1)}, u32[]{:S(2)}, u32[]{:S(2)}) %all-to-all-start.1) | async-done | bytes 1048608 | tf_op jit(solution)/shard_map/all_to_all | solution.py:364
  188.2 2.4 %collective-permute-start.20 = (bf16[64,2048]{1,0:T(8,128)(2,1)S(1)}, bf16[64,2048]{1,0:T(8,128)(2,1)S(1)}, u32[]{:S(2)}, u32[]{:S(2)}) collective-permute-start(bf16[64,2048]{1,0:T(8,128)(2,1)S(1)} %get-tuple-element.130), channel_id=1, source_target_pairs={{0,3},{1,0},{2,1},{3,2},{4,7},{5,4},{6,5},{7,6},{8,11},{9,8},{10,9... | collective-permute-start | bytes 786440 | tf_op jit(solution)/shard_map/ppermute | solution.py:17
  190.6 1.6 add_convert_fusion
  193.3 4.7 %collective-permute-done.18 = bf16[64,2048]{1,0:T(8,128)(2,1)S(1)} collective-permute-done((bf16[64,2048]{1,0:T(8,128)(2,1)S(1)}, bf16[64,2048]{1,0:T(8,128)(2,1)S(1)}, u32[]{:S(2)}, u32[]{:S(2)}) %collective-permute-start.18) | collective-permute-done | bytes 262176 | tf_op jit(solution)/shard_map/ppermute | solution.py:17
  198.0 4.6 %collective-permute-done.19 = bf16[64,2048]{1,0:T(8,128)(2,1)S(1)} collective-permute-done((bf16[64,2048]{1,0:T(8,128)(2,1)S(1)}, bf16[64,2048]{1,0:T(8,128)(2,1)S(1)}, u32[]{:S(2)}, u32[]{:S(2)}) %collective-permute-start.19) | collective-permute-done | bytes 262176 | tf_op jit(solution)/shard_map/ppermute | solution.py:17
  (106 shorter events, 30.1 us)
Async XLA Ops:
  0.6 63.8 %copy-start = (bf16[512,2048]{1,0:T(8,128)(2,1)S(1)}, bf16[512,2048]{1,0:T(8,128)(2,1)}, u32[]{:S(2)}) copy-start(bf16[512,2048]{1,0:T(8,128)(2,1)} %param.16) | copy-start | bytes 6291460
  3.0 14.0 %collective-permute-start.2 = (bf16[64,2048]{1,0:T(8,128)(2,1)S(1)}, bf16[64,2048]{1,0:T(8,128)(2,1)S(1)}, u32[]{:S(2)}, u32[]{:S(2)}) collective-permute-start(bf16[64,2048]{1,0:T(8,128)(2,1)S(1)} %fusion.7.refs_0_), channel_id=1, source_target_pairs={{0,1},{1,2},{2,3},{3,0},{4,5},{5,6},{6,7},{7,4},{8,9},{9,10},{10,1... | collective-permute-start | bytes 786440 | tf_op jit(solution)/shard_map/ppermute | solution.py:17
  4.7 14.5 %collective-permute-start.1 = (bf16[64,2048]{1,0:T(8,128)(2,1)S(1)}, bf16[64,2048]{1,0:T(8,128)(2,1)S(1)}, u32[]{:S(2)}, u32[]{:S(2)}) collective-permute-start(bf16[64,2048]{1,0:T(8,128)(2,1)S(1)} %fusion.7.refs_0_), channel_id=1, source_target_pairs={{0,2},{1,3},{2,0},{3,1},{4,6},{5,7},{6,4},{7,5},{8,10},{9,11},{10,... | collective-permute-start | bytes 786440 | tf_op jit(solution)/shard_map/ppermute | solution.py:17
  7.6 11.6 %collective-permute-start = (bf16[64,2048]{1,0:T(8,128)(2,1)S(1)}, bf16[64,2048]{1,0:T(8,128)(2,1)S(1)}, u32[]{:S(2)}, u32[]{:S(2)}) collective-permute-start(bf16[64,2048]{1,0:T(8,128)(2,1)S(1)} %fusion.7.refs_0_), channel_id=1, source_target_pairs={{0,3},{1,0},{2,1},{3,2},{4,7},{5,4},{6,5},{7,6},{8,11},{9,8},{10,9... | collective-permute-start | bytes 786440 | tf_op jit(solution)/shard_map/ppermute | solution.py:17
  9.7 7.3 %collective-permute-start.3 = (bf16[32,512]{1,0:T(8,128)(2,1)S(1)}, bf16[32,512]{1,0:T(8,128)(2,1)S(1)}, u32[]{:S(2)}, u32[]{:S(2)}) collective-permute-start(bf16[32,512]{1,0:T(8,128)(2,1)S(1)} %slice.3), channel_id=1, source_target_pairs={{0,4},{4,8},{8,12},{12,16},{16,20},{20,24},{24,28},{28,32},{32,36}... | collective-permute-start | bytes 98312 | tf_op jit(solution)/shard_map/ppermute | solution.py:12
  16.3 16.0 %copy-start.16 = (bf16[31,512]{1,0:T(8,128)(2,1)S(1)}, bf16[31,512]{1,0:T(8,128)(2,1)}, u32[]{:S(2)}) copy-start(bf16[31,512]{1,0:T(8,128)(2,1)} %taps_ref.1) | copy-start | bytes 95236
  20.6 39.5 %all-to-all-start = ((bf16[64,4,2048]{2,1,0:T(4,128)(2,1)}), bf16[64,4,2048]{2,1,0:T(4,128)(2,1)S(1)}, u32[]{:S(2)}, u32[]{:S(2)}) async-start(bf16[64,4,2048]{2,1,0:T(4,128)(2,1)} %copy-done.7), calls=%async_computation | async-start | bytes 2097152 | tf_op jit(solution)/shard_map/all_to_all | solution.py:303
  52.4 1.7 copy-start.24
  52.4 1.7 copy-start.25
  60.1 11.9 %copy-start.5 = (bf16[1,512,2048]{2,1,0:T(8,128)(2,1)S(1)}, bf16[1,512,2048]{2,1,0:T(8,128)(2,1)}, u32[]{:S(2)}) copy-start(bf16[1,512,2048]{2,1,0:T(8,128)(2,1)} %down_ref.7) | copy-start | bytes 6291460
  61.2 16.2 %collective-permute-start.4 = (bf16[128,2048]{1,0:T(8,128)(2,1)}, bf16[128,2048]{1,0:T(8,128)(2,1)S(1)}, u32[]{:S(2)}, u32[]{:S(2)}) collective-permute-start(bf16[128,2048]{1,0:T(8,128)(2,1)} %get-tuple-element.88.top_ref), channel_id=1, source_target_pairs={{0,1},{1,2},{2,3},{3,0},{4,5},{5,6},{6,7},{7,4},{8,9},{9,10},{10,1... | collective-permute-start | bytes 1572872 | tf_op jit(solution)/shard_map/ppermute | solution.py:17
  62.4 9.6 %copy-start.1 = (bf16[1,2048,512]{2,1,0:T(8,128)(2,1)S(1)}, bf16[1,2048,512]{2,1,0:T(8,128)(2,1)}, u32[]{:S(2)}) copy-start(bf16[1,2048,512]{2,1,0:T(8,128)(2,1)} %gate_ref.7) | copy-start | bytes 6291460
  62.4 9.6 %copy-start.3 = (bf16[1,2048,512]{2,1,0:T(8,128)(2,1)S(1)}, bf16[1,2048,512]{2,1,0:T(8,128)(2,1)}, u32[]{:S(2)}) copy-start(bf16[1,2048,512]{2,1,0:T(8,128)(2,1)} %up_ref.7) | copy-start | bytes 6291460
  62.4 15.0 %collective-permute-start.5 = (bf16[128,2048]{1,0:T(8,128)(2,1)}, bf16[128,2048]{1,0:T(8,128)(2,1)S(1)}, u32[]{:S(2)}, u32[]{:S(2)}) collective-permute-start(bf16[128,2048]{1,0:T(8,128)(2,1)} %get-tuple-element.89.low_ref), channel_id=1, source_target_pairs={{0,3},{1,0},{2,1},{3,2},{4,7},{5,4},{6,5},{7,6},{8,11},{9,8},{10,9... | collective-permute-start | bytes 1572872 | tf_op jit(solution)/shard_map/ppermute | solution.py:17
  66.6 49.8 %collective-permute-start.13 = (bf16[128,2048]{1,0:T(8,128)(2,1)}, bf16[128,2048]{1,0:T(8,128)(2,1)}, u32[]{:S(2)}, u32[]{:S(2)}) collective-permute-start(bf16[128,2048]{1,0:T(8,128)(2,1)} %convolution_convert_fusion), channel_id=1, source_target_pairs={{0,3},{1,0},{2,1},{3,2},{4,7},{5,4},{6,5},{7,6},{8,11},{9,8},{10,9... | collective-permute-start | bytes 1572872 | tf_op jit(solution)/shard_map/ppermute | solution.py:17
  70.0 8.8 %copy-start.17 = (bf16[1024,512]{1,0:T(8,128)(2,1)S(1)}, bf16[1024,512]{1,0:T(8,128)(2,1)}, u32[]{:S(2)}) copy-start(bf16[1024,512]{1,0:T(8,128)(2,1)} %multiply_convert_fusion) | copy-start | bytes 3145732
  70.0 30.0 %collective-permute-start.8 = (bf16[128,2048]{1,0:T(8,128)(2,1)}, bf16[128,2048]{1,0:T(8,128)(2,1)}, u32[]{:S(2)}, u32[]{:S(2)}) collective-permute-start(bf16[128,2048]{1,0:T(8,128)(2,1)} %get-tuple-element.88.top_ref), channel_id=1, source_target_pairs={{0,3},{1,0},{2,1},{3,2},{4,7},{5,4},{6,5},{7,6},{8,11},{9,8},{10,9... | collective-permute-start | bytes 1572872 | tf_op jit(solution)/shard_map/ppermute | solution.py:17
  70.9 30.4 %collective-permute-start.9 = (bf16[128,2048]{1,0:T(8,128)(2,1)}, bf16[128,2048]{1,0:T(8,128)(2,1)}, u32[]{:S(2)}, u32[]{:S(2)}) collective-permute-start(bf16[128,2048]{1,0:T(8,128)(2,1)} %get-tuple-element.89.low_ref), channel_id=1, source_target_pairs={{0,1},{1,2},{2,3},{3,0},{4,5},{5,6},{6,7},{7,4},{8,9},{9,10},{10,1... | collective-permute-start | bytes 1572872 | tf_op jit(solution)/shard_map/ppermute | solution.py:17
  75.9 5.3 %copy-start.11 = (bf16[128,2048]{1,0:T(8,128)(2,1)}, bf16[128,2048]{1,0:T(8,128)(2,1)S(1)}, u32[]{:S(2)}) copy-start(bf16[128,2048]{1,0:T(8,128)(2,1)S(1)} %get-tuple-element.91.refs_0_) | copy-start | bytes 1572868
  75.9 5.3 %copy-start.13 = (bf16[128,2048]{1,0:T(8,128)(2,1)}, bf16[128,2048]{1,0:T(8,128)(2,1)S(1)}, u32[]{:S(2)}) copy-start(bf16[128,2048]{1,0:T(8,128)(2,1)S(1)} %get-tuple-element.116.refs_3_) | copy-start | bytes 1572868
  77.4 29.8 %collective-permute-start.6 = (bf16[128,2048]{1,0:T(8,128)(2,1)S(1)}, bf16[128,2048]{1,0:T(8,128)(2,1)}, u32[]{:S(2)}, u32[]{:S(2)}) collective-permute-start(bf16[128,2048]{1,0:T(8,128)(2,1)S(1)} %collective-permute-done.4.top_ref), channel_id=1, source_target_pairs={{0,1},{1,2},{2,3},{3,0},{4,5},{5,6},{6,7},{7,4},{8,9},{9,10},{10,1... | collective-permute-start | bytes 1572872 | tf_op jit(solution)/shard_map/ppermute | solution.py:17
  83.7 2.5 %copy-start.23 = (s32[256,2]{0,1:T(2,128)S(1)}, s32[256,2]{0,1:T(2,128)}, u32[]{:S(2)}) copy-start(s32[256,2]{0,1:T(2,128)} %param.19) | copy-start | bytes 6148
  83.7 2.5 %copy-start.26 = (f32[256,2]{0,1:T(2,128)S(1)}, f32[256,2]{0,1:T(2,128)}, u32[]{:S(2)}) copy-start(f32[256,2]{0,1:T(2,128)} %param.20) | copy-start | bytes 6148
  87.3 23.9 %collective-permute-start.7 = (bf16[128,2048]{1,0:T(8,128)(2,1)S(1)}, bf16[128,2048]{1,0:T(8,128)(2,1)S(1)}, u32[]{:S(2)}, u32[]{:S(2)}) collective-permute-start(bf16[128,2048]{1,0:T(8,128)(2,1)S(1)} %collective-permute-done.5.low_ref), channel_id=1, source_target_pairs={{0,3},{1,0},{2,1},{3,2},{4,7},{5,4},{6,5},{7,6},{8,11},{9,8},{10,9... | collective-permute-start | bytes 1572872 | tf_op jit(solution)/shard_map/ppermute | solution.py:17
  89.2 1.6 copy-start.2
  94.0 2.9 %copy-start.21 = (f32[256,256]{1,0:T(8,128)S(1)}, f32[256,256]{1,0:T(8,128)}, u32[]{:S(2)}) copy-start(f32[256,256]{1,0:T(8,128)} %reshape.29) | copy-start | bytes 786436
  94.0 6.0 %copy-start.22 = (bf16[128,2048]{1,0:T(8,128)(2,1)S(1)}, bf16[128,2048]{1,0:T(8,128)(2,1)}, u32[]{:S(2)}) copy-start(bf16[128,2048]{1,0:T(8,128)(2,1)} %convolution_convert_fusion.1) | copy-start | bytes 1572868
  100.0 20.3 %collective-permute-start.12 = (bf16[128,2048]{1,0:T(8,128)(2,1)S(1)}, bf16[128,2048]{1,0:T(8,128)(2,1)S(1)}, u32[]{:S(2)}, u32[]{:S(2)}) collective-permute-start(bf16[128,2048]{1,0:T(8,128)(2,1)S(1)} %copy-done.22), channel_id=1, source_target_pairs={{0,1},{1,2},{2,3},{3,0},{4,5},{5,6},{6,7},{7,4},{8,9},{9,10},{10,1... | collective-permute-start | bytes 1572872 | tf_op jit(solution)/shard_map/ppermute | solution.py:17
  101.3 37.3 %collective-permute-start.15 = (bf16[128,2048]{1,0:T(8,128)(2,1)S(1)}, bf16[128,2048]{1,0:T(8,128)(2,1)S(1)}, u32[]{:S(2)}, u32[]{:S(2)}) collective-permute-start(bf16[128,2048]{1,0:T(8,128)(2,1)S(1)} %get-tuple-element.115), channel_id=1, source_target_pairs={{0,3},{1,0},{2,1},{3,2},{4,7},{5,4},{6,5},{7,6},{8,11},{9,8},{10,9... | collective-permute-start | bytes 1572872 | tf_op jit(solution)/shard_map/ppermute | solution.py:17
  107.3 31.3 %collective-permute-start.16 = (bf16[128,2048]{1,0:T(8,128)(2,1)S(1)}, bf16[128,2048]{1,0:T(8,128)(2,1)S(1)}, u32[]{:S(2)}, u32[]{:S(2)}) collective-permute-start(bf16[128,2048]{1,0:T(8,128)(2,1)S(1)} %get-tuple-element.117), channel_id=1, source_target_pairs={{0,1},{1,2},{2,3},{3,0},{4,5},{5,6},{6,7},{7,4},{8,9},{9,10},{10,1... | collective-permute-start | bytes 1572872 | tf_op jit(solution)/shard_map/ppermute | solution.py:17
  111.1 7.2 %copy-start.18 = (bf16[128,2048]{1,0:T(8,128)(2,1)S(1)}, bf16[128,2048]{1,0:T(8,128)(2,1)}, u32[]{:S(2)}) copy-start(bf16[128,2048]{1,0:T(8,128)(2,1)} %convolution_convert_fusion.4) | copy-start | bytes 1572868
  111.1 9.2 %copy-start.19 = (bf16[128,2048]{1,0:T(8,128)(2,1)S(1)}, bf16[128,2048]{1,0:T(8,128)(2,1)}, u32[]{:S(2)}) copy-start(bf16[128,2048]{1,0:T(8,128)(2,1)} %convolution_convert_fusion.7) | copy-start | bytes 1572868
  115.0 20.9 %collective-permute-start.10 = (bf16[128,2048]{1,0:T(8,128)(2,1)S(1)}, bf16[128,2048]{1,0:T(8,128)(2,1)S(1)}, u32[]{:S(2)}, u32[]{:S(2)}) collective-permute-start(bf16[128,2048]{1,0:T(8,128)(2,1)S(1)} %get-tuple-element.110), channel_id=1, source_target_pairs={{0,1},{1,2},{2,3},{3,0},{4,5},{5,6},{6,7},{7,4},{8,9},{9,10},{10,1... | collective-permute-start | bytes 1572872 | tf_op jit(solution)/shard_map/ppermute | solution.py:17
  116.4 19.5 %collective-permute-start.11 = (bf16[128,2048]{1,0:T(8,128)(2,1)S(1)}, bf16[128,2048]{1,0:T(8,128)(2,1)S(1)}, u32[]{:S(2)}, u32[]{:S(2)}) collective-permute-start(bf16[128,2048]{1,0:T(8,128)(2,1)S(1)} %get-tuple-element.111), channel_id=1, source_target_pairs={{0,3},{1,0},{2,1},{3,2},{4,7},{5,4},{6,5},{7,6},{8,11},{9,8},{10,9... | collective-permute-start | bytes 1572872 | tf_op jit(solution)/shard_map/ppermute | solution.py:17
  120.3 30.0 %copy-start.12 = (bf16[128,2048]{1,0:T(8,128)(2,1)S(1)}, bf16[128,2048]{1,0:T(8,128)(2,1)}, u32[]{:S(2)}) copy-start(bf16[128,2048]{1,0:T(8,128)(2,1)} %copy-done.11) | copy-start | bytes 1572868
  120.3 30.0 %copy-start.14 = (bf16[128,2048]{1,0:T(8,128)(2,1)S(1)}, bf16[128,2048]{1,0:T(8,128)(2,1)}, u32[]{:S(2)}) copy-start(bf16[128,2048]{1,0:T(8,128)(2,1)} %copy-done.13) | copy-start | bytes 1572868
  136.0 11.6 %collective-permute-start.17 = (bf16[128,2048]{1,0:T(8,128)(2,1)S(1)}, bf16[128,2048]{1,0:T(8,128)(2,1)S(1)}, u32[]{:S(2)}, u32[]{:S(2)}) collective-permute-start(bf16[128,2048]{1,0:T(8,128)(2,1)S(1)} %add_convert_fusion.2), channel_id=1, source_target_pairs={{0,3},{1,0},{2,1},{3,2},{4,7},{5,4},{6,5},{7,6},{8,11},{9,8},{10,9... | collective-permute-start | bytes 1572872 | tf_op jit(solution)/shard_map/ppermute | solution.py:17
  138.2 12.1 %collective-permute-start.14 = (bf16[128,2048]{1,0:T(8,128)(2,1)S(1)}, bf16[128,2048]{1,0:T(8,128)(2,1)S(1)}, u32[]{:S(2)}, u32[]{:S(2)}) collective-permute-start(bf16[128,2048]{1,0:T(8,128)(2,1)S(1)} %add_convert_fusion.3), channel_id=1, source_target_pairs={{0,1},{1,2},{2,3},{3,0},{4,5},{5,6},{6,7},{7,4},{8,9},{9,10},{10,1... | collective-permute-start | bytes 1572872 | tf_op jit(solution)/shard_map/ppermute | solution.py:17
  151.8 34.4 %copy-start.10 = (bf16[256,256]{1,0:T(8,128)(2,1)S(1)}, bf16[256,256]{1,0:T(8,128)(2,1)}, u32[]{:S(2)}) copy-start(bf16[256,256]{1,0:T(8,128)(2,1)} %get-tuple-element.125.refs_0_) | copy-start | bytes 393220
  151.8 34.4 %all-to-all-start.1 = ((bf16[64,4,2048]{2,1,0:T(4,128)(2,1)}), bf16[64,4,2048]{2,1,0:T(4,128)(2,1)S(1)}, u32[]{:S(2)}, u32[]{:S(2)}) async-start(bf16[64,4,2048]{2,1,0:T(4,128)(2,1)} %copy-done.8), calls=%async_computation.1 | async-start | bytes 2097152 | tf_op jit(solution)/shard_map/all_to_all | solution.py:364
  158.3 16.3 %collective-permute-start.21 = (bf16[128,2048]{1,0:T(8,128)(2,1)}, bf16[128,2048]{1,0:T(8,128)(2,1)S(1)}, u32[]{:S(2)}, u32[]{:S(2)}) collective-permute-start(bf16[128,2048]{1,0:T(8,128)(2,1)} %add_convert_fusion.5), channel_id=1, source_target_pairs={{0,1},{1,2},{2,3},{3,0},{4,5},{5,6},{6,7},{7,4},{8,9},{9,10},{10,1... | collective-permute-start | bytes 1572872 | tf_op jit(solution)/shard_map/ppermute | solution.py:17
  158.4 16.2 %collective-permute-start.22 = (bf16[128,2048]{1,0:T(8,128)(2,1)}, bf16[128,2048]{1,0:T(8,128)(2,1)S(1)}, u32[]{:S(2)}, u32[]{:S(2)}) collective-permute-start(bf16[128,2048]{1,0:T(8,128)(2,1)} %convolution_convert_fusion.5), channel_id=1, source_target_pairs={{0,3},{1,0},{2,1},{3,2},{4,7},{5,4},{6,5},{7,6},{8,11},{9,8},{10,9... | collective-permute-start | bytes 1572872 | tf_op jit(solution)/shard_map/ppermute | solution.py:17
  161.6 29.0 %collective-permute-start.23 = (bf16[128,2048]{1,0:T(8,128)(2,1)}, bf16[128,2048]{1,0:T(8,128)(2,1)}, u32[]{:S(2)}, u32[]{:S(2)}) collective-permute-start(bf16[128,2048]{1,0:T(8,128)(2,1)} %convolution_convert_fusion.6), channel_id=1, source_target_pairs={{0,1},{1,2},{2,3},{3,0},{4,5},{5,6},{6,7},{7,4},{8,9},{9,10},{10,1... | collective-permute-start | bytes 1572872 | tf_op jit(solution)/shard_map/ppermute | solution.py:17
  161.6 29.0 %collective-permute-start.24 = (bf16[128,2048]{1,0:T(8,128)(2,1)}, bf16[128,2048]{1,0:T(8,128)(2,1)}, u32[]{:S(2)}, u32[]{:S(2)}) collective-permute-start(bf16[128,2048]{1,0:T(8,128)(2,1)} %add_convert_fusion.4), channel_id=1, source_target_pairs={{0,3},{1,0},{2,1},{3,2},{4,7},{5,4},{6,5},{7,6},{8,11},{9,8},{10,9... | collective-permute-start | bytes 1572872 | tf_op jit(solution)/shard_map/ppermute | solution.py:17
  186.2 6.0 %copy-start.20 = (bf16[128,2048]{1,0:T(8,128)(2,1)S(1)}, bf16[128,2048]{1,0:T(8,128)(2,1)}, u32[]{:S(2)}) copy-start(bf16[128,2048]{1,0:T(8,128)(2,1)} %add_convert_fusion.1) | copy-start | bytes 1572868
  187.2 10.8 %collective-permute-start.18 = (bf16[64,2048]{1,0:T(8,128)(2,1)S(1)}, bf16[64,2048]{1,0:T(8,128)(2,1)S(1)}, u32[]{:S(2)}, u32[]{:S(2)}) collective-permute-start(bf16[64,2048]{1,0:T(8,128)(2,1)S(1)} %get-tuple-element.128), channel_id=1, source_target_pairs={{0,2},{1,3},{2,0},{3,1},{4,6},{5,7},{6,4},{7,5},{8,10},{9,11},{10,... | collective-permute-start | bytes 786440 | tf_op jit(solution)/shard_map/ppermute | solution.py:17
  187.3 15.4 %collective-permute-start.19 = (bf16[64,2048]{1,0:T(8,128)(2,1)S(1)}, bf16[64,2048]{1,0:T(8,128)(2,1)S(1)}, u32[]{:S(2)}, u32[]{:S(2)}) collective-permute-start(bf16[64,2048]{1,0:T(8,128)(2,1)S(1)} %get-tuple-element.129), channel_id=1, source_target_pairs={{0,1},{1,2},{2,3},{3,0},{4,5},{5,6},{6,7},{7,4},{8,9},{9,10},{10,1... | collective-permute-start | bytes 786440 | tf_op jit(solution)/shard_map/ppermute | solution.py:17
  188.2 14.4 %collective-permute-start.20 = (bf16[64,2048]{1,0:T(8,128)(2,1)S(1)}, bf16[64,2048]{1,0:T(8,128)(2,1)S(1)}, u32[]{:S(2)}, u32[]{:S(2)}) collective-permute-start(bf16[64,2048]{1,0:T(8,128)(2,1)S(1)} %get-tuple-element.130), channel_id=1, source_target_pairs={{0,3},{1,0},{2,1},{3,2},{4,7},{5,4},{6,5},{7,6},{8,11},{9,8},{10,9... | collective-permute-start | bytes 786440 | tf_op jit(solution)/shard_map/ppermute | solution.py:17
  (6 other events, 7.7 us)

commit v2 on v1

--- a/solution.py
+++ b/solution.py
@@ -161,6 +161,21 @@
     )(rows, history, taps)
 
 
+def norm_body(rows_ref, gain_ref, out_ref):
+    rows = rows_ref[...].astype(jnp.float32)
+    mean = jnp.mean(rows * rows, axis=1, keepdims=True)
+    out_ref[...] = (rows * lax.rsqrt(mean + 1e-06) * gain_ref[...]).astype(jnp.bfloat16)
+
+
+def normalized(rows, gain):
+    return pl.pallas_call(
+        norm_body,
+        out_shape=jax.ShapeDtypeStruct(rows.shape, jnp.bfloat16),
+        compiler_params=pltpu.CompilerParams(vmem_limit_bytes=10 * 1024 * 1024),
+        name="norm",
+    )(rows, gain[None])
+
+
 def pick_body(select_ref, *refs):
     pieces, out_ref, group = refs[:-2], refs[-2], refs[-1]
     own = pieces[0].shape[0]
@@ -269,12 +284,7 @@
     share = capacity // tp_count
     slots = ep_count * share
 
-    moe_float = moe_input.astype(jnp.float32)
-    normed = (
-        moe_float
-        * lax.rsqrt(jnp.mean(moe_float * moe_float, axis=1, keepdims=True) + 1e-06)
-        * moe_gain
-    ).astype(jnp.bfloat16)
+    normed = normalized(moe_input, moe_gain)
     normed, conv_input = tied(normed, conv_input)
     pieces = (normed, turned(normed, -1), turned(normed, 2), turned(normed, 1))
     history = shifted(conv_input[conv_input.shape[0] - 32 :], "ep", 1)
@@ -305,7 +315,11 @@
     local_rows, local_width = conv_input.shape
     mixed, *stats = convolved(conv_input, history, conv_kernel)
     full_width = local_width * tp_count
-    sums, squares = lax.psum(tuple(stats), "tp")
+    stats = jnp.concatenate(stats, axis=0)
+    for pairs in (((0, 1), (2, 3)), ((0, 3), (1, 2))):
+        swapped = [*pairs, *((to, source) for source, to in pairs)]
+        stats = stats + lax.ppermute(stats, "tp", swapped)
+    sums, squares = jnp.split(stats, 2, axis=0)
     center = sums / full_width
     spread = jnp.maximum(squares / full_width - center * center, 0.0)
     factor = lax.rsqrt(spread + 1e-05)

time: 206 us -> 205 us (level)
  blocking collectives: 9.98 us -> 0 us
  waiting for transfers between devices: 69.8 us -> 76.2 us
  starting transfers between devices: 54.8 us -> 58.2 us
  other arithmetic: 15.7 us -> 13.4 us
    psum x1 -> x0, blocking collectives: 9.98 us -> none  [local(): sums, squares = lax.psum(tuple(stats), 'tp')]
    ppermute x0 -> x2, waiting for transfers between devices: none -> 3.42 us  [local(): stats = stats + lax.ppermute(stats, 'tp', swapped)]
    ppermute x0 -> x2, starting transfers between devices: none -> 3.4 us  [local(): stats = stats + lax.ppermute(stats, 'tp', swapped)]
    all_to_all x1, waiting for transfers between devices: 4.15 us -> 7.34 us  [local(): landed = lax.all_to_all(rows, 'ep', split_axis=0, concat_axis=0, tiled=True)]
    unnamed x54 -> x59, local copies, waits for them, and re-layouts: 9.37 us -> 11.2 us
  transfers between devices with their start and end apart: 27 -> 29, of which waited for: 13 -> 15; matrix products, arithmetic and copies ran while one was open for 15% -> 15% of each run, Pallas kernels for 11% -> 11%
where the time goes in v2:
time: 205 us; the launch traced here: 203 us
  waiting for transfers between devices  76.2 us (37%)
  starting transfers between devices  58.2 us (28%)
  Pallas kernels  25.1 us (12%)
  local copies, waits for them, and re-layouts  17 us (8%)
  other arithmetic  13.4 us (7%)
  matrix products  12 us (6%)
    ppermute x24, waiting for transfers between devices, turned(): lax.ppermute(value, 'tp', [(i, (i + steps) % count) for i in range(count)])  55.2 us
    ppermute x24, starting transfers between devices, turned(): lax.ppermute(value, 'tp', [(i, (i + steps) % count) for i in range(count)])  34.8 us
    pallas_call x4, Pallas kernels, expert(): pl.pallas_call(expert_body, grid=(steps,), in_specs=[block, block, pl.Blo...  14.5 us
    dot_general x9, matrix products, dot(): return jnp.dot(lhs, rhs, preferred_element_type=jnp.float32)  12 us
    all_to_all x1, starting transfers between devices, local(): landed = lax.all_to_all(rows, 'ep', split_axis=0, concat_axis=0, tiled=True)  11.6 us
    unnamed x59, local copies, waits for them, and re-layouts  11.2 us
    all_to_all x1, waiting for transfers between devices, local(): lax.all_to_all(totals, 'ep', split_axis=0, concat_axis=0, tiled=True)  9.53 us
    convert_element_type x7, other arithmetic, rounded_sum(): sum((value.astype(jnp.float32) for value in values)).astype(jnp.bfloat16)  7.66 us
  transfers between devices with their start and end apart: 29, of which 15 were waited for; matrix products, arithmetic and copies ran while one was open for 15% of the time, Pallas kernels for 11%

profile of v2, /device:TPU:32, one launch (start us, length us, event | category | flops | bytes accessed | tf_op | source)
XLA Modules:
  0.0 202.9 jit_solution(3755635388185390811)
XLA Ops:
  2.6 1.7 collective-permute-start.2
  4.3 2.9 %collective-permute-start.1 = (bf16[64,2048]{1,0:T(8,128)(2,1)S(1)}, bf16[64,2048]{1,0:T(8,128)(2,1)S(1)}, u32[]{:S(2)}, u32[]{:S(2)}) collective-permute-start(bf16[64,2048]{1,0:T(8,128)(2,1)S(1)} %norm.1.refs_0_), channel_id=1, source_target_pairs={{0,2},{1,3},{2,0},{3,1},{4,6},{5,7},{6,4},{7,5},{8,10},{9,11},{10,... | collective-permute-start | bytes 786440 | tf_op jit(solution)/shard_map/ppermute | solution.py:17
  7.2 1.3 collective-permute-start
  9.3 1.9 collective-permute-start.3
  13.1 1.7 eq.50
  16.6 2.2 %collective-permute-done.1.refs_2_ = bf16[64,2048]{1,0:T(8,128)(2,1)S(1)} collective-permute-done((bf16[64,2048]{1,0:T(8,128)(2,1)S(1)}, bf16[64,2048]{1,0:T(8,128)(2,1)S(1)}, u32[]{:S(2)}, u32[]{:S(2)}) %collective-permute-start.1) | collective-permute-done | bytes 262176 | tf_op jit(solution)/shard_map/ppermute | solution.py:17
  20.2 11.6 %all-to-all-start = ((bf16[64,4,2048]{2,1,0:T(4,128)(2,1)}), bf16[64,4,2048]{2,1,0:T(4,128)(2,1)S(1)}, u32[]{:S(2)}, u32[]{:S(2)}) async-start(bf16[64,4,2048]{2,1,0:T(4,128)(2,1)} %copy-done.7), calls=%async_computation | async-start | bytes 2097152 | tf_op jit(solution)/shard_map/all_to_all | solution.py:313
  33.1 7.5 %taps.1 = (f32[4,1024,128]{2,1,0:T(8,128)S(1)}, f32[8,128]{1,0:T(8,128)S(1)}, f32[8,128]{1,0:T(8,128)S(1)}) custom-call(bf16[1024,512]{1,0:T(8,128)(2,1)S(1)} %copy-done.17, bf16[32,512]{1,0:T(8,128)(2,1)S(1)} %collective-permute-done.3.history_ref, bf16[31,512]{1,0:T(8,128)(2,1)S(1)} %copy-done.18), custom_call_target="tpu_custom_call" | custom-call | flops 6501171200 | bytes 3145728 | tf_op jit(solution)/shard_map/taps/pallas_call | solution.py:147
  40.6 1.4 copy-done.9
  43.2 2.4 %collective-permute-done.4 = f32[16,128]{1,0:T(8,128)S(1)} collective-permute-done((f32[16,128]{1,0:T(8,128)S(1)}, f32[16,128]{1,0:T(8,128)S(1)}, u32[]{:S(2)}, u32[]{:S(2)}) %collective-permute-start.4) | collective-permute-done | bytes 8224 | tf_op jit(solution)/shard_map/ppermute | solution.py:321
  45.6 2.2 %collective-permute-start.5 = (f32[16,128]{1,0:T(8,128)S(1)}, f32[16,128]{1,0:T(8,128)S(1)}, u32[]{:S(2)}, u32[]{:S(2)}) collective-permute-start(f32[16,128]{1,0:T(8,128)S(1)} %add.118), channel_id=1, source_target_pairs={{0,3},{1,2},{3,0},{2,1},{4,7},{5,6},{7,4},{6,5},{8,11},{9,10},{11,... | collective-permute-start | bytes 24584 | tf_op jit(solution)/shard_map/ppermute | solution.py:321
  47.8 1.7 slice_bitcast_fusion.3
  50.5 1.9 multiply_convert_fusion
  52.4 7.3 %all-to-all-done.whole_ref = bf16[64,4,2048]{2,1,0:T(4,128)(2,1)S(1)} async-done(((bf16[64,4,2048]{2,1,0:T(4,128)(2,1)}), bf16[64,4,2048]{2,1,0:T(4,128)(2,1)S(1)}, u32[]{:S(2)}, u32[]{:S(2)}) %all-to-all-start) | async-done | bytes 1048608 | tf_op jit(solution)/shard_map/all_to_all | solution.py:313
  62.1 2.0 collective-permute-start.7
  64.1 2.1 %convolution_convert_fusion = bf16[128,2048]{1,0:T(8,128)(2,1)} fusion(bf16[512,2048]{1,0:T(8,128)(2,1)S(1)} %copy-done, bf16[1024,512]{1,0:T(8,128)(2,1)} %multiply_convert_fusion, s32[]{:T(128)S(6)} %select_n.46), kind=kOutput, calls=%fused_computation | convolution fusion | flops 268697600 | bytes 2752516 | tf_op jit(solution)/shard_map/dot_general | solution.py:21
  67.5 2.1 %convolution_convert_fusion.1 = bf16[128,2048]{1,0:T(8,128)(2,1)} fusion(bf16[512,2048]{1,0:T(8,128)(2,1)S(1)} %copy-done, bf16[1024,512]{1,0:T(8,128)(2,1)} %multiply_convert_fusion, s32[]{:T(128)S(6)} %select_n.45), kind=kOutput, calls=%fused_computation.1 | convolution fusion | flops 268697600 | bytes 2752516 | tf_op jit(solution)/shard_map/dot_general | solution.py:21
  71.6 3.9 %expert.4 = (bf16[128,2048]{1,0:T(8,128)(2,1)S(1)}, bf16[128,2048]{1,0:T(8,128)(2,1)S(1)}) custom-call(bf16[128,2048]{1,0:T(8,128)(2,1)} %get-tuple-element.88.top_ref, bf16[128,2048]{1,0:T(8,128)(2,1)} %get-tuple-element.89.low_ref, bf16[1,2048,512]{2,1,0:T(8,128)(2,1)S(1)} %copy-done.1, bf16[1,2048,512]{2,1,0:T(8,128)(2,1)S(1)} %copy-done.3, ...), custom_call_target="tpu_custom_call" | custom-call | flops 1610612736 | bytes 8388608 | tf_op jit(solution)/shard_map/expert/pallas_call | solution.py:71
  75.6 1.5 collective-permute-done.6.top_ref
  84.6 1.3 convolution_convert_fusion.7
  86.9 1.9 collective-permute-start.9
  88.9 1.6 copy-done.2
  90.5 1.6 copy-done.4
  92.1 1.6 copy-done.6
  93.7 2.8 %expert.5 = (bf16[128,2048]{1,0:T(8,128)(2,1)S(1)}, bf16[128,2048]{1,0:T(8,128)(2,1)S(1)}) custom-call(bf16[128,2048]{1,0:T(8,128)(2,1)S(1)} %collective-permute-done.6.top_ref, bf16[128,2048]{1,0:T(8,128)(2,1)S(1)} %collective-permute-done.7.low_ref, bf16[1,2048,512]{2,1,0:T(8,128)(2,1)S(1)} %copy-done.2, bf16[1,2048,512]{2,1,0:T(8,128)(2,1)S(1)} %copy-done.4, ...), custom_call_target="tpu_custom_call" | custom-call | flops 1610612736 | bytes 8388608 | tf_op jit(solution)/shard_map/expert/pallas_call | solution.py:71
  97.2 2.4 %collective-permute-done.10.top_ref = bf16[128,2048]{1,0:T(8,128)(2,1)} collective-permute-done((bf16[128,2048]{1,0:T(8,128)(2,1)}, bf16[128,2048]{1,0:T(8,128)(2,1)}, u32[]{:S(2)}, u32[]{:S(2)}) %collective-permute-start.10) | collective-permute-done | bytes 524320 | tf_op jit(solution)/shard_map/ppermute | solution.py:17
  99.7 1.3 collective-permute-start.14
  100.9 2.0 collective-permute-start.17
  102.9 3.9 %expert.6 = (bf16[128,2048]{1,0:T(8,128)(2,1)S(1)}, bf16[128,2048]{1,0:T(8,128)(2,1)S(1)}) custom-call(bf16[128,2048]{1,0:T(8,128)(2,1)} %collective-permute-done.10.top_ref, bf16[128,2048]{1,0:T(8,128)(2,1)} %collective-permute-done.11.low_ref, bf16[1,2048,512]{2,1,0:T(8,128)(2,1)S(1)} %copy-done.2, bf16[1,2048,512]{2,1,0:T(8,128)(2,1)S(1)} %copy-done.4, ...), custom_call_target="tpu_custom_call" | custom-call | flops 1610612736 | bytes 8388608 | tf_op jit(solution)/shard_map/expert/pallas_call | solution.py:71
  107.0 3.8 %collective-permute-done.9.low_ref = bf16[128,2048]{1,0:T(8,128)(2,1)S(1)} collective-permute-done((bf16[128,2048]{1,0:T(8,128)(2,1)S(1)}, bf16[128,2048]{1,0:T(8,128)(2,1)S(1)}, u32[]{:S(2)}, u32[]{:S(2)}) %collective-permute-start.9) | collective-permute-done | bytes 524320 | tf_op jit(solution)/shard_map/ppermute | solution.py:17
  110.8 3.8 %expert.7 = (bf16[128,2048]{1,0:T(8,128)(2,1)S(1)}, bf16[128,2048]{1,0:T(8,128)(2,1)S(1)}) custom-call(bf16[128,2048]{1,0:T(8,128)(2,1)} %collective-permute-done.8.top_ref, bf16[128,2048]{1,0:T(8,128)(2,1)S(1)} %collective-permute-done.9.low_ref, bf16[1,2048,512]{2,1,0:T(8,128)(2,1)S(1)} %copy-done.2, bf16[1,2048,512]{2,1,0:T(8,128)(2,1)S(1)} %copy-done.4, ...), custom_call_target="tpu_custom_call" | custom-call | flops 1610612736 | bytes 8388608 | tf_op jit(solution)/shard_map/expert/pallas_call | solution.py:71
  114.6 1.6 collective-permute-start.12
  116.2 2.0 collective-permute-start.13
  118.2 2.0 add_convert_fusion.4
  121.1 14.4 %collective-permute-done.12 = bf16[128,2048]{1,0:T(8,128)(2,1)S(1)} collective-permute-done((bf16[128,2048]{1,0:T(8,128)(2,1)S(1)}, bf16[128,2048]{1,0:T(8,128)(2,1)S(1)}, u32[]{:S(2)}, u32[]{:S(2)}) %collective-permute-start.12) | collective-permute-done | bytes 524320 | tf_op jit(solution)/shard_map/ppermute | solution.py:17
  135.7 1.8 collective-permute-start.19
  138.0 9.1 %collective-permute-done.19.refs_5_ = bf16[128,2048]{1,0:T(8,128)(2,1)S(1)} collective-permute-done((bf16[128,2048]{1,0:T(8,128)(2,1)S(1)}, bf16[128,2048]{1,0:T(8,128)(2,1)S(1)}, u32[]{:S(2)}, u32[]{:S(2)}) %collective-permute-start.19) | collective-permute-done | bytes 524320 | tf_op jit(solution)/shard_map/ppermute | solution.py:17
  147.1 2.7 %collective-permute-done.16.refs_1_ = bf16[128,2048]{1,0:T(8,128)(2,1)S(1)} collective-permute-done((bf16[128,2048]{1,0:T(8,128)(2,1)S(1)}, bf16[128,2048]{1,0:T(8,128)(2,1)S(1)}, u32[]{:S(2)}, u32[]{:S(2)}) %collective-permute-start.16) | collective-permute-done | bytes 524320 | tf_op jit(solution)/shard_map/ppermute | solution.py:17
  151.2 6.5 %all-to-all-start.1 = ((bf16[64,4,2048]{2,1,0:T(4,128)(2,1)}), bf16[64,4,2048]{2,1,0:T(4,128)(2,1)S(1)}, u32[]{:S(2)}, u32[]{:S(2)}) async-start(bf16[64,4,2048]{2,1,0:T(4,128)(2,1)} %copy-done.8), calls=%async_computation.1 | async-start | bytes 2097152 | tf_op jit(solution)/shard_map/all_to_all | solution.py:378
  157.8 3.2 %collective-permute-start.24 = (bf16[128,2048]{1,0:T(8,128)(2,1)}, bf16[128,2048]{1,0:T(8,128)(2,1)S(1)}, u32[]{:S(2)}, u32[]{:S(2)}) collective-permute-start(bf16[128,2048]{1,0:T(8,128)(2,1)} %convolution_convert_fusion.5), channel_id=1, source_target_pairs={{0,3},{1,0},{2,1},{3,2},{4,7},{5,4},{6,5},{7,6},{8,11},{9,8},{10,9... | collective-permute-start | bytes 1572872 | tf_op jit(solution)/shard_map/ppermute | solution.py:17
  161.0 3.2 %collective-permute-start.26 = (bf16[128,2048]{1,0:T(8,128)(2,1)}, bf16[128,2048]{1,0:T(8,128)(2,1)}, u32[]{:S(2)}, u32[]{:S(2)}) collective-permute-start(bf16[128,2048]{1,0:T(8,128)(2,1)} %add_convert_fusion.4), channel_id=1, source_target_pairs={{0,3},{1,0},{2,1},{3,2},{4,7},{5,4},{6,5},{7,6},{8,11},{9,8},{10,9... | collective-permute-start | bytes 1572872 | tf_op jit(solution)/shard_map/ppermute | solution.py:17
  164.2 9.7 %collective-permute-done.23 = bf16[128,2048]{1,0:T(8,128)(2,1)S(1)} collective-permute-done((bf16[128,2048]{1,0:T(8,128)(2,1)}, bf16[128,2048]{1,0:T(8,128)(2,1)S(1)}, u32[]{:S(2)}, u32[]{:S(2)}) %collective-permute-start.23) | collective-permute-done | bytes 524320 | tf_op jit(solution)/shard_map/ppermute | solution.py:17
  174.0 2.1 %add_convert_fusion.1 = bf16[128,2048]{1,0:T(8,128)(2,1)} fusion(bf16[128,2048]{1,0:T(8,128)(2,1)S(1)} %collective-permute-done.24, bf16[128,2048]{1,0:T(8,128)(2,1)S(1)} %collective-permute-done.23, bf16[128,2048]{1,0:T(8,128)(2,1)} %convolution_convert_fusion.3), kind=kLoop, calls=%fused_computation.18 | loop fusion | flops 1572864 | bytes 2097152 | tf_op jit(solution)/shard_map/convert_element_type | solution.py:37
  176.1 9.5 %all-to-all-done.1.returned_ref = bf16[64,4,2048]{2,1,0:T(4,128)(2,1)S(1)} async-done(((bf16[64,4,2048]{2,1,0:T(4,128)(2,1)}), bf16[64,4,2048]{2,1,0:T(4,128)(2,1)S(1)}, u32[]{:S(2)}, u32[]{:S(2)}) %all-to-all-start.1) | async-done | bytes 1048608 | tf_op jit(solution)/shard_map/all_to_all | solution.py:378
  187.6 2.4 %collective-permute-start.22 = (bf16[64,2048]{1,0:T(8,128)(2,1)S(1)}, bf16[64,2048]{1,0:T(8,128)(2,1)S(1)}, u32[]{:S(2)}, u32[]{:S(2)}) collective-permute-start(bf16[64,2048]{1,0:T(8,128)(2,1)S(1)} %get-tuple-element.130), channel_id=1, source_target_pairs={{0,3},{1,0},{2,1},{3,2},{4,7},{5,4},{6,5},{7,6},{8,11},{9,8},{10,9... | collective-permute-start | bytes 786440 | tf_op jit(solution)/shard_map/ppermute | solution.py:17
  190.0 1.6 add_convert_fusion
  192.7 4.7 %collective-permute-done.20 = bf16[64,2048]{1,0:T(8,128)(2,1)S(1)} collective-permute-done((bf16[64,2048]{1,0:T(8,128)(2,1)S(1)}, bf16[64,2048]{1,0:T(8,128)(2,1)S(1)}, u32[]{:S(2)}, u32[]{:S(2)}) %collective-permute-start.20) | collective-permute-done | bytes 262176 | tf_op jit(solution)/shard_map/ppermute | solution.py:17
  197.4 4.7 %collective-permute-done.21 = bf16[64,2048]{1,0:T(8,128)(2,1)S(1)} collective-permute-done((bf16[64,2048]{1,0:T(8,128)(2,1)S(1)}, bf16[64,2048]{1,0:T(8,128)(2,1)S(1)}, u32[]{:S(2)}, u32[]{:S(2)}) %collective-permute-start.21) | collective-permute-done | bytes 262176 | tf_op jit(solution)/shard_map/ppermute | solution.py:17
  (115 shorter events, 33.3 us)
Async XLA Ops:
  0.6 63.4 %copy-start = (bf16[512,2048]{1,0:T(8,128)(2,1)S(1)}, bf16[512,2048]{1,0:T(8,128)(2,1)}, u32[]{:S(2)}) copy-start(bf16[512,2048]{1,0:T(8,128)(2,1)} %param.16) | copy-start | bytes 6291460
  2.6 14.0 %collective-permute-start.2 = (bf16[64,2048]{1,0:T(8,128)(2,1)S(1)}, bf16[64,2048]{1,0:T(8,128)(2,1)S(1)}, u32[]{:S(2)}, u32[]{:S(2)}) collective-permute-start(bf16[64,2048]{1,0:T(8,128)(2,1)S(1)} %norm.1.refs_0_), channel_id=1, source_target_pairs={{0,1},{1,2},{2,3},{3,0},{4,5},{5,6},{6,7},{7,4},{8,9},{9,10},{10,1... | collective-permute-start | bytes 786440 | tf_op jit(solution)/shard_map/ppermute | solution.py:17
  4.3 14.5 %collective-permute-start.1 = (bf16[64,2048]{1,0:T(8,128)(2,1)S(1)}, bf16[64,2048]{1,0:T(8,128)(2,1)S(1)}, u32[]{:S(2)}, u32[]{:S(2)}) collective-permute-start(bf16[64,2048]{1,0:T(8,128)(2,1)S(1)} %norm.1.refs_0_), channel_id=1, source_target_pairs={{0,2},{1,3},{2,0},{3,1},{4,6},{5,7},{6,4},{7,5},{8,10},{9,11},{10,... | collective-permute-start | bytes 786440 | tf_op jit(solution)/shard_map/ppermute | solution.py:17
  7.2 11.6 %collective-permute-start = (bf16[64,2048]{1,0:T(8,128)(2,1)S(1)}, bf16[64,2048]{1,0:T(8,128)(2,1)S(1)}, u32[]{:S(2)}, u32[]{:S(2)}) collective-permute-start(bf16[64,2048]{1,0:T(8,128)(2,1)S(1)} %norm.1.refs_0_), channel_id=1, source_target_pairs={{0,3},{1,0},{2,1},{3,2},{4,7},{5,4},{6,5},{7,6},{8,11},{9,8},{10,9... | collective-permute-start | bytes 786440 | tf_op jit(solution)/shard_map/ppermute | solution.py:17
  9.3 7.3 %collective-permute-start.3 = (bf16[32,512]{1,0:T(8,128)(2,1)S(1)}, bf16[32,512]{1,0:T(8,128)(2,1)S(1)}, u32[]{:S(2)}, u32[]{:S(2)}) collective-permute-start(bf16[32,512]{1,0:T(8,128)(2,1)S(1)} %slice.3), channel_id=1, source_target_pairs={{0,4},{4,8},{8,12},{12,16},{16,20},{20,24},{24,28},{28,32},{32,36}... | collective-permute-start | bytes 98312 | tf_op jit(solution)/shard_map/ppermute | solution.py:12
  15.9 16.0 %copy-start.18 = (bf16[31,512]{1,0:T(8,128)(2,1)S(1)}, bf16[31,512]{1,0:T(8,128)(2,1)}, u32[]{:S(2)}) copy-start(bf16[31,512]{1,0:T(8,128)(2,1)} %taps_ref.1) | copy-start | bytes 95236
  20.2 39.5 %all-to-all-start = ((bf16[64,4,2048]{2,1,0:T(4,128)(2,1)}), bf16[64,4,2048]{2,1,0:T(4,128)(2,1)S(1)}, u32[]{:S(2)}, u32[]{:S(2)}) async-start(bf16[64,4,2048]{2,1,0:T(4,128)(2,1)} %copy-done.7), calls=%async_computation | async-start | bytes 2097152 | tf_op jit(solution)/shard_map/all_to_all | solution.py:313
  41.9 3.7 %collective-permute-start.4 = (f32[16,128]{1,0:T(8,128)S(1)}, f32[16,128]{1,0:T(8,128)S(1)}, u32[]{:S(2)}, u32[]{:S(2)}) collective-permute-start(f32[16,128]{1,0:T(8,128)S(1)} %constant_dynamic-update-slice_fusion), channel_id=1, source_target_pairs={{0,1},{2,3},{1,0},{3,2},{4,5},{6,7},{5,4},{7,6},{8,9},{10,11},{9,8... | collective-permute-start | bytes 24584 | tf_op jit(solution)/shard_map/ppermute | solution.py:321
  45.6 4.9 %collective-permute-start.5 = (f32[16,128]{1,0:T(8,128)S(1)}, f32[16,128]{1,0:T(8,128)S(1)}, u32[]{:S(2)}, u32[]{:S(2)}) collective-permute-start(f32[16,128]{1,0:T(8,128)S(1)} %add.118), channel_id=1, source_target_pairs={{0,3},{1,2},{3,0},{2,1},{4,7},{5,6},{7,4},{6,5},{8,11},{9,10},{11,... | collective-permute-start | bytes 24584 | tf_op jit(solution)/shard_map/ppermute | solution.py:321
  47.8 2.7 %copy-start.26 = (f32[512]{0:T(512)S(1)}, f32[512]{0:T(512)}, u32[]{:S(2)}) copy-start(f32[512]{0:T(512)} %param.15) | copy-start | bytes 6148
  47.8 2.7 %copy-start.27 = (f32[512]{0:T(512)S(1)}, f32[512]{0:T(512)}, u32[]{:S(2)}) copy-start(f32[512]{0:T(512)} %param.14) | copy-start | bytes 6148
  59.7 11.9 %copy-start.5 = (bf16[1,512,2048]{2,1,0:T(8,128)(2,1)S(1)}, bf16[1,512,2048]{2,1,0:T(8,128)(2,1)}, u32[]{:S(2)}) copy-start(bf16[1,512,2048]{2,1,0:T(8,128)(2,1)} %down_ref.7) | copy-start | bytes 6291460
  60.8 16.2 %collective-permute-start.6 = (bf16[128,2048]{1,0:T(8,128)(2,1)}, bf16[128,2048]{1,0:T(8,128)(2,1)S(1)}, u32[]{:S(2)}, u32[]{:S(2)}) collective-permute-start(bf16[128,2048]{1,0:T(8,128)(2,1)} %get-tuple-element.88.top_ref), channel_id=1, source_target_pairs={{0,1},{1,2},{2,3},{3,0},{4,5},{5,6},{6,7},{7,4},{8,9},{9,10},{10,1... | collective-permute-start | bytes 1572872 | tf_op jit(solution)/shard_map/ppermute | solution.py:17
  62.1 9.6 %copy-start.1 = (bf16[1,2048,512]{2,1,0:T(8,128)(2,1)S(1)}, bf16[1,2048,512]{2,1,0:T(8,128)(2,1)}, u32[]{:S(2)}) copy-start(bf16[1,2048,512]{2,1,0:T(8,128)(2,1)} %gate_ref.7) | copy-start | bytes 6291460
  62.1 9.6 %copy-start.3 = (bf16[1,2048,512]{2,1,0:T(8,128)(2,1)S(1)}, bf16[1,2048,512]{2,1,0:T(8,128)(2,1)}, u32[]{:S(2)}) copy-start(bf16[1,2048,512]{2,1,0:T(8,128)(2,1)} %up_ref.7) | copy-start | bytes 6291460
  62.1 15.0 %collective-permute-start.7 = (bf16[128,2048]{1,0:T(8,128)(2,1)}, bf16[128,2048]{1,0:T(8,128)(2,1)S(1)}, u32[]{:S(2)}, u32[]{:S(2)}) collective-permute-start(bf16[128,2048]{1,0:T(8,128)(2,1)} %get-tuple-element.89.low_ref), channel_id=1, source_target_pairs={{0,3},{1,0},{2,1},{3,2},{4,7},{5,4},{6,5},{7,6},{8,11},{9,8},{10,9... | collective-permute-start | bytes 1572872 | tf_op jit(solution)/shard_map/ppermute | solution.py:17
  66.2 50.0 %collective-permute-start.15 = (bf16[128,2048]{1,0:T(8,128)(2,1)}, bf16[128,2048]{1,0:T(8,128)(2,1)}, u32[]{:S(2)}, u32[]{:S(2)}) collective-permute-start(bf16[128,2048]{1,0:T(8,128)(2,1)} %convolution_convert_fusion), channel_id=1, source_target_pairs={{0,3},{1,0},{2,1},{3,2},{4,7},{5,4},{6,5},{7,6},{8,11},{9,8},{10,9... | collective-permute-start | bytes 1572872 | tf_op jit(solution)/shard_map/ppermute | solution.py:17
  69.6 8.8 %copy-start.19 = (bf16[1024,512]{1,0:T(8,128)(2,1)S(1)}, bf16[1024,512]{1,0:T(8,128)(2,1)}, u32[]{:S(2)}) copy-start(bf16[1024,512]{1,0:T(8,128)(2,1)} %multiply_convert_fusion) | copy-start | bytes 3145732
  69.6 30.0 %collective-permute-start.10 = (bf16[128,2048]{1,0:T(8,128)(2,1)}, bf16[128,2048]{1,0:T(8,128)(2,1)}, u32[]{:S(2)}, u32[]{:S(2)}) collective-permute-start(bf16[128,2048]{1,0:T(8,128)(2,1)} %get-tuple-element.88.top_ref), channel_id=1, source_target_pairs={{0,3},{1,0},{2,1},{3,2},{4,7},{5,4},{6,5},{7,6},{8,11},{9,8},{10,9... | collective-permute-start | bytes 1572872 | tf_op jit(solution)/shard_map/ppermute | solution.py:17
  70.6 30.4 %collective-permute-start.11 = (bf16[128,2048]{1,0:T(8,128)(2,1)}, bf16[128,2048]{1,0:T(8,128)(2,1)}, u32[]{:S(2)}, u32[]{:S(2)}) collective-permute-start(bf16[128,2048]{1,0:T(8,128)(2,1)} %get-tuple-element.89.low_ref), channel_id=1, source_target_pairs={{0,1},{1,2},{2,3},{3,0},{4,5},{5,6},{6,7},{7,4},{8,9},{9,10},{10,1... | collective-permute-start | bytes 1572872 | tf_op jit(solution)/shard_map/ppermute | solution.py:17
  75.6 5.3 %copy-start.11 = (bf16[128,2048]{1,0:T(8,128)(2,1)}, bf16[128,2048]{1,0:T(8,128)(2,1)S(1)}, u32[]{:S(2)}) copy-start(bf16[128,2048]{1,0:T(8,128)(2,1)S(1)} %get-tuple-element.91.refs_0_) | copy-start | bytes 1572868
  75.6 5.3 %copy-start.13 = (bf16[128,2048]{1,0:T(8,128)(2,1)}, bf16[128,2048]{1,0:T(8,128)(2,1)S(1)}, u32[]{:S(2)}) copy-start(bf16[128,2048]{1,0:T(8,128)(2,1)S(1)} %get-tuple-element.116.refs_3_) | copy-start | bytes 1572868
  77.1 29.8 %collective-permute-start.8 = (bf16[128,2048]{1,0:T(8,128)(2,1)S(1)}, bf16[128,2048]{1,0:T(8,128)(2,1)}, u32[]{:S(2)}, u32[]{:S(2)}) collective-permute-start(bf16[128,2048]{1,0:T(8,128)(2,1)S(1)} %collective-permute-done.6.top_ref), channel_id=1, source_target_pairs={{0,1},{1,2},{2,3},{3,0},{4,5},{5,6},{6,7},{7,4},{8,9},{9,10},{10,1... | collective-permute-start | bytes 1572872 | tf_op jit(solution)/shard_map/ppermute | solution.py:17
  83.4 2.6 %copy-start.28 = (f32[256,2]{0,1:T(2,128)S(1)}, f32[256,2]{0,1:T(2,128)}, u32[]{:S(2)}) copy-start(f32[256,2]{0,1:T(2,128)} %param.20) | copy-start | bytes 6148
  86.9 23.8 %collective-permute-start.9 = (bf16[128,2048]{1,0:T(8,128)(2,1)S(1)}, bf16[128,2048]{1,0:T(8,128)(2,1)S(1)}, u32[]{:S(2)}, u32[]{:S(2)}) collective-permute-start(bf16[128,2048]{1,0:T(8,128)(2,1)S(1)} %collective-permute-done.7.low_ref), channel_id=1, source_target_pairs={{0,3},{1,0},{2,1},{3,2},{4,7},{5,4},{6,5},{7,6},{8,11},{9,8},{10,9... | collective-permute-start | bytes 1572872 | tf_op jit(solution)/shard_map/ppermute | solution.py:17
  93.6 2.9 %copy-start.23 = (f32[256,256]{1,0:T(8,128)S(1)}, f32[256,256]{1,0:T(8,128)}, u32[]{:S(2)}) copy-start(f32[256,256]{1,0:T(8,128)} %reshape.20) | copy-start | bytes 786436
  93.6 6.0 %copy-start.24 = (bf16[128,2048]{1,0:T(8,128)(2,1)S(1)}, bf16[128,2048]{1,0:T(8,128)(2,1)}, u32[]{:S(2)}) copy-start(bf16[128,2048]{1,0:T(8,128)(2,1)} %convolution_convert_fusion.1) | copy-start | bytes 1572868
  99.7 20.5 %collective-permute-start.14 = (bf16[128,2048]{1,0:T(8,128)(2,1)S(1)}, bf16[128,2048]{1,0:T(8,128)(2,1)S(1)}, u32[]{:S(2)}, u32[]{:S(2)}) collective-permute-start(bf16[128,2048]{1,0:T(8,128)(2,1)S(1)} %copy-done.24), channel_id=1, source_target_pairs={{0,1},{1,2},{2,3},{3,0},{4,5},{5,6},{6,7},{7,4},{8,9},{9,10},{10,1... | collective-permute-start | bytes 1572872 | tf_op jit(solution)/shard_map/ppermute | solution.py:17
  100.9 37.0 %collective-permute-start.17 = (bf16[128,2048]{1,0:T(8,128)(2,1)S(1)}, bf16[128,2048]{1,0:T(8,128)(2,1)S(1)}, u32[]{:S(2)}, u32[]{:S(2)}) collective-permute-start(bf16[128,2048]{1,0:T(8,128)(2,1)S(1)} %get-tuple-element.115), channel_id=1, source_target_pairs={{0,3},{1,0},{2,1},{3,2},{4,7},{5,4},{6,5},{7,6},{8,11},{9,8},{10,9... | collective-permute-start | bytes 1572872 | tf_op jit(solution)/shard_map/ppermute | solution.py:17
  106.9 31.1 %collective-permute-start.18 = (bf16[128,2048]{1,0:T(8,128)(2,1)S(1)}, bf16[128,2048]{1,0:T(8,128)(2,1)S(1)}, u32[]{:S(2)}, u32[]{:S(2)}) collective-permute-start(bf16[128,2048]{1,0:T(8,128)(2,1)S(1)} %get-tuple-element.117), channel_id=1, source_target_pairs={{0,1},{1,2},{2,3},{3,0},{4,5},{5,6},{6,7},{7,4},{8,9},{9,10},{10,1... | collective-permute-start | bytes 1572872 | tf_op jit(solution)/shard_map/ppermute | solution.py:17
  110.8 7.4 %copy-start.20 = (bf16[128,2048]{1,0:T(8,128)(2,1)S(1)}, bf16[128,2048]{1,0:T(8,128)(2,1)}, u32[]{:S(2)}) copy-start(bf16[128,2048]{1,0:T(8,128)(2,1)} %convolution_convert_fusion.4) | copy-start | bytes 1572868
  110.8 9.4 %copy-start.21 = (bf16[128,2048]{1,0:T(8,128)(2,1)S(1)}, bf16[128,2048]{1,0:T(8,128)(2,1)}, u32[]{:S(2)}) copy-start(bf16[128,2048]{1,0:T(8,128)(2,1)} %convolution_convert_fusion.7) | copy-start | bytes 1572868
  114.6 20.9 %collective-permute-start.12 = (bf16[128,2048]{1,0:T(8,128)(2,1)S(1)}, bf16[128,2048]{1,0:T(8,128)(2,1)S(1)}, u32[]{:S(2)}, u32[]{:S(2)}) collective-permute-start(bf16[128,2048]{1,0:T(8,128)(2,1)S(1)} %get-tuple-element.110), channel_id=1, source_target_pairs={{0,1},{1,2},{2,3},{3,0},{4,5},{5,6},{6,7},{7,4},{8,9},{9,10},{10,1... | collective-permute-start | bytes 1572872 | tf_op jit(solution)/shard_map/ppermute | solution.py:17
  116.2 19.3 %collective-permute-start.13 = (bf16[128,2048]{1,0:T(8,128)(2,1)S(1)}, bf16[128,2048]{1,0:T(8,128)(2,1)S(1)}, u32[]{:S(2)}, u32[]{:S(2)}) collective-permute-start(bf16[128,2048]{1,0:T(8,128)(2,1)S(1)} %get-tuple-element.111), channel_id=1, source_target_pairs={{0,3},{1,0},{2,1},{3,2},{4,7},{5,4},{6,5},{7,6},{8,11},{9,8},{10,9... | collective-permute-start | bytes 1572872 | tf_op jit(solution)/shard_map/ppermute | solution.py:17
  120.2 29.6 %copy-start.12 = (bf16[128,2048]{1,0:T(8,128)(2,1)S(1)}, bf16[128,2048]{1,0:T(8,128)(2,1)}, u32[]{:S(2)}) copy-start(bf16[128,2048]{1,0:T(8,128)(2,1)} %copy-done.11) | copy-start | bytes 1572868
  120.2 29.6 %copy-start.14 = (bf16[128,2048]{1,0:T(8,128)(2,1)S(1)}, bf16[128,2048]{1,0:T(8,128)(2,1)}, u32[]{:S(2)}) copy-start(bf16[128,2048]{1,0:T(8,128)(2,1)} %copy-done.13) | copy-start | bytes 1572868
  135.7 11.4 %collective-permute-start.19 = (bf16[128,2048]{1,0:T(8,128)(2,1)S(1)}, bf16[128,2048]{1,0:T(8,128)(2,1)S(1)}, u32[]{:S(2)}, u32[]{:S(2)}) collective-permute-start(bf16[128,2048]{1,0:T(8,128)(2,1)S(1)} %add_convert_fusion.2), channel_id=1, source_target_pairs={{0,3},{1,0},{2,1},{3,2},{4,7},{5,4},{6,5},{7,6},{8,11},{9,8},{10,9... | collective-permute-start | bytes 1572872 | tf_op jit(solution)/shard_map/ppermute | solution.py:17
  137.6 12.1 %collective-permute-start.16 = (bf16[128,2048]{1,0:T(8,128)(2,1)S(1)}, bf16[128,2048]{1,0:T(8,128)(2,1)S(1)}, u32[]{:S(2)}, u32[]{:S(2)}) collective-permute-start(bf16[128,2048]{1,0:T(8,128)(2,1)S(1)} %add_convert_fusion.3), channel_id=1, source_target_pairs={{0,1},{1,2},{2,3},{3,0},{4,5},{5,6},{6,7},{7,4},{8,9},{9,10},{10,1... | collective-permute-start | bytes 1572872 | tf_op jit(solution)/shard_map/ppermute | solution.py:17
  151.2 34.4 %copy-start.10 = (bf16[256,256]{1,0:T(8,128)(2,1)S(1)}, bf16[256,256]{1,0:T(8,128)(2,1)}, u32[]{:S(2)}) copy-start(bf16[256,256]{1,0:T(8,128)(2,1)} %get-tuple-element.125.refs_0_) | copy-start | bytes 393220
  151.2 34.4 %all-to-all-start.1 = ((bf16[64,4,2048]{2,1,0:T(4,128)(2,1)}), bf16[64,4,2048]{2,1,0:T(4,128)(2,1)S(1)}, u32[]{:S(2)}, u32[]{:S(2)}) async-start(bf16[64,4,2048]{2,1,0:T(4,128)(2,1)} %copy-done.8), calls=%async_computation.1 | async-start | bytes 2097152 | tf_op jit(solution)/shard_map/all_to_all | solution.py:378
  157.7 16.3 %collective-permute-start.23 = (bf16[128,2048]{1,0:T(8,128)(2,1)}, bf16[128,2048]{1,0:T(8,128)(2,1)S(1)}, u32[]{:S(2)}, u32[]{:S(2)}) collective-permute-start(bf16[128,2048]{1,0:T(8,128)(2,1)} %add_convert_fusion.5), channel_id=1, source_target_pairs={{0,1},{1,2},{2,3},{3,0},{4,5},{5,6},{6,7},{7,4},{8,9},{9,10},{10,1... | collective-permute-start | bytes 1572872 | tf_op jit(solution)/shard_map/ppermute | solution.py:17
  157.8 16.2 %collective-permute-start.24 = (bf16[128,2048]{1,0:T(8,128)(2,1)}, bf16[128,2048]{1,0:T(8,128)(2,1)S(1)}, u32[]{:S(2)}, u32[]{:S(2)}) collective-permute-start(bf16[128,2048]{1,0:T(8,128)(2,1)} %convolution_convert_fusion.5), channel_id=1, source_target_pairs={{0,3},{1,0},{2,1},{3,2},{4,7},{5,4},{6,5},{7,6},{8,11},{9,8},{10,9... | collective-permute-start | bytes 1572872 | tf_op jit(solution)/shard_map/ppermute | solution.py:17
  161.0 29.0 %collective-permute-start.25 = (bf16[128,2048]{1,0:T(8,128)(2,1)}, bf16[128,2048]{1,0:T(8,128)(2,1)}, u32[]{:S(2)}, u32[]{:S(2)}) collective-permute-start(bf16[128,2048]{1,0:T(8,128)(2,1)} %convolution_convert_fusion.6), channel_id=1, source_target_pairs={{0,1},{1,2},{2,3},{3,0},{4,5},{5,6},{6,7},{7,4},{8,9},{9,10},{10,1... | collective-permute-start | bytes 1572872 | tf_op jit(solution)/shard_map/ppermute | solution.py:17
  161.0 29.0 %collective-permute-start.26 = (bf16[128,2048]{1,0:T(8,128)(2,1)}, bf16[128,2048]{1,0:T(8,128)(2,1)}, u32[]{:S(2)}, u32[]{:S(2)}) collective-permute-start(bf16[128,2048]{1,0:T(8,128)(2,1)} %add_convert_fusion.4), channel_id=1, source_target_pairs={{0,3},{1,0},{2,1},{3,2},{4,7},{5,4},{6,5},{7,6},{8,11},{9,8},{10,9... | collective-permute-start | bytes 1572872 | tf_op jit(solution)/shard_map/ppermute | solution.py:17
  185.6 6.0 %copy-start.22 = (bf16[128,2048]{1,0:T(8,128)(2,1)S(1)}, bf16[128,2048]{1,0:T(8,128)(2,1)}, u32[]{:S(2)}) copy-start(bf16[128,2048]{1,0:T(8,128)(2,1)} %add_convert_fusion.1) | copy-start | bytes 1572868
  186.6 10.8 %collective-permute-start.20 = (bf16[64,2048]{1,0:T(8,128)(2,1)S(1)}, bf16[64,2048]{1,0:T(8,128)(2,1)S(1)}, u32[]{:S(2)}, u32[]{:S(2)}) collective-permute-start(bf16[64,2048]{1,0:T(8,128)(2,1)S(1)} %get-tuple-element.128), channel_id=1, source_target_pairs={{0,2},{1,3},{2,0},{3,1},{4,6},{5,7},{6,4},{7,5},{8,10},{9,11},{10,... | collective-permute-start | bytes 786440 | tf_op jit(solution)/shard_map/ppermute | solution.py:17
  186.7 15.4 %collective-permute-start.21 = (bf16[64,2048]{1,0:T(8,128)(2,1)S(1)}, bf16[64,2048]{1,0:T(8,128)(2,1)S(1)}, u32[]{:S(2)}, u32[]{:S(2)}) collective-permute-start(bf16[64,2048]{1,0:T(8,128)(2,1)S(1)} %get-tuple-element.129), channel_id=1, source_target_pairs={{0,1},{1,2},{2,3},{3,0},{4,5},{5,6},{6,7},{7,4},{8,9},{9,10},{10,1... | collective-permute-start | bytes 786440 | tf_op jit(solution)/shard_map/ppermute | solution.py:17
  187.6 14.4 %collective-permute-start.22 = (bf16[64,2048]{1,0:T(8,128)(2,1)S(1)}, bf16[64,2048]{1,0:T(8,128)(2,1)S(1)}, u32[]{:S(2)}, u32[]{:S(2)}) collective-permute-start(bf16[64,2048]{1,0:T(8,128)(2,1)S(1)} %get-tuple-element.130), channel_id=1, source_target_pairs={{0,3},{1,0},{2,1},{3,2},{4,7},{5,4},{6,5},{7,6},{8,11},{9,8},{10,9... | collective-permute-start | bytes 786440 | tf_op jit(solution)/shard_map/ppermute | solution.py:17
  (10 other events, 13.7 us)
